TPU v7x, 128 devices: a whole 4x4x4 slice. The times are simulated.
128 devices in a mesh: ep: 32 (over z, y, core), tp: 4 (over x).
Axes of the slice: x: 4, y: 4, z: 4, core: 2. Of those that a mesh axis runs over, the one named last changes fastest.
Arguments:
- query_rows: bfloat16 [16384, 1024], P('ep', 'tp'), may hold values from -60 to 60
- key_rows: bfloat16 [16384, 1024], P('ep', 'tp'), may hold values from -6 to 6
- value_rows: bfloat16 [16384, 1024], P('ep', 'tp'), may hold values from -6 to 6
- lambdas: float32 [8], P('tp'), may hold values from 0.3 to 0.8
- out_gain: float32 [128], replicated, may hold values from 0.1 to 1.9
- out_weight: bfloat16 [1024, 2048], P('tp'), may hold values from -0.1875 to 0.1875
- tokens: bfloat16 [16384, 2048], P(('ep', 'tp')), may hold values from -6 to 6
- norm_gain: float32 [2048], replicated, may hold values from 0.1 to 1.9
- group_ids: int32 [16384], P(('ep', 'tp')), may hold values from 0 to 3, as said below
- inner_ids: int32 [16384, 2], P(('ep', 'tp')), may hold values from 0 to 7, as said below
- route_weights: float32 [16384, 2], P(('ep', 'tp')), may hold values from 0.2 to 1
- gate_weight: bfloat16 [32, 2048, 1024], P('ep', None, 'tp'), may hold values from -0.125 to 0.125
- up_weight: bfloat16 [32, 2048, 1024], P('ep', None, 'tp'), may hold values from -0.125 to 0.125
- down_weight: bfloat16 [32, 1024, 2048], P('ep', 'tp'), may hold values from -0.1875 to 0.1875
Outputs:
- attended: bfloat16 [16384, 2048], P(('ep', 'tp'))
- combined: bfloat16 [16384, 2048], P(('ep', 'tp'))
Inputs may be any that keep to these rules, and one draw needn't show every extreme that they name: In the 128 rows of one device no expert group_ids * 8 + inner_ids is named more than 10 times; some expert is named exactly 10 times in the rows of every device. `inner_ids`: the 2 entries of a row are different.
All inputs are finite; a program needn't handle non-finite values.
Results may differ from a plain program's by a relative error of at most 0.013.
Values may be sent and summed in bfloat16 or wider, within the bound.
A program may use at most 128 MiB of HBM per device.

v0:
```python
import jax
import jax.numpy as jnp
from jax import lax
from jax.sharding import PartitionSpec as P

GROUPS = 4


eps = 1e-06
neg_big = -1e30


def from_partner(block, axis, stride):
    count = lax.axis_size(axis)
    route = []
    for low in range(count):
        high = low | 1 << stride
        if high != low and high < count:
            route += [(low, high), (high, low)]
    return lax.ppermute(block, axis, route)


def sent_together(arrays, axis, dim, along):
    widths = [a.shape[along] for a in arrays]
    both = jnp.concatenate(arrays, axis=along)
    out = lax.all_gather(both, axis, axis=dim, tiled=True)
    return tuple(jnp.split(out, [sum(widths[:k]) for k in range(1, len(widths))], axis=along))


def body(
    query_rows,
    key_rows,
    value_rows,
    lambdas,
    out_gain,
    out_weight,
    tokens,
    norm_gain,
    group_ids,
    inner_ids,
    route_weights,
    gate_weight,
    up_weight,
    down_weight,
):
    seg_rows = query_rows.shape[0]
    heads_here = lambdas.shape[0]
    value_dim = out_gain.shape[0]
    query_dim = query_rows.shape[1] // (2 * heads_here)
    tok_dev = tokens.shape[0]
    model_width = tokens.shape[1]
    topk_count = inner_ids.shape[1]
    experts = lax.axis_size("ep")
    ep_index = lax.axis_index("ep")
    group_size = experts // GROUPS
    capacity = 5 * tok_dev * topk_count // (4 * experts)
    half_rows = seg_rows // 2
    bit_count = experts.bit_length() - 1

    def heads_first(rows_block):
        count = rows_block.shape[0]
        return rows_block.reshape(count, heads_here, 2, query_dim).transpose(1, 2, 0, 3)

    late_part = query_rows[half_rows:]
    for bit in range(bit_count):
        late_part = from_partner(late_part, "ep", bit)
    mirror = experts - 1 - ep_index
    query_groups = (
        (
            heads_first(query_rows[:half_rows]),
            ep_index * seg_rows + jnp.arange(half_rows, dtype=jnp.int32),
        ),
        (
            heads_first(late_part),
            mirror * seg_rows + half_rows + jnp.arange(half_rows, dtype=jnp.int32),
        ),
    )
    score_scale = query_dim ** (-0.5)

    def one_map(state, query_map, key_map, value_blk, allowed):
        top_old, total_old, accum_old = state
        scores = (
            jnp.einsum("hqd,hdk->hqk", query_map, key_map, preferred_element_type=jnp.float32)
            * score_scale
        )
        scores = jnp.where(allowed[None, :, :], scores, neg_big)
        top_new = jnp.maximum(top_old, jnp.max(scores, axis=2))
        exps = jnp.where(allowed[None, :, :], jnp.exp(scores - top_new[:, :, None]), 0.0)
        fade = jnp.exp(top_old - top_new)
        total_new = total_old * fade + jnp.sum(exps, axis=2)
        accum_new = accum_old * fade[:, :, None] + jnp.einsum(
            "hqk,hdk->hqd", exps.astype(jnp.bfloat16), value_blk, preferred_element_type=jnp.float32
        )
        return (top_new, total_new, accum_new)

    def key_block(running, query_part, query_pos, key_blk, value_blk, key_start):
        key_pos = key_start + jnp.arange(key_blk.shape[3], dtype=jnp.int32)
        allowed = key_pos[None, :] <= query_pos[:, None]
        first_state = one_map(running[:3], query_part[:, 0], key_blk[:, 0], value_blk, allowed)
        second_state = one_map(running[3:], query_part[:, 1], key_blk[:, 1], value_blk, allowed)
        return first_state + second_state

    def initial(rows):
        top_init = jnp.full((heads_here, rows), neg_big, jnp.float32)
        total_init = jnp.zeros((heads_here, rows), jnp.float32)
        accum_init = jnp.zeros((heads_here, rows, value_dim), jnp.float32)
        return (top_init, total_init, accum_init, top_init, total_init, accum_init)

    def finish(state):
        first_out = state[2] / state[1][:, :, None]
        second_out = state[5] / state[4][:, :, None]
        heads_out = first_out - lambdas[:, None, None] * second_out
        mean_sq = jnp.mean(heads_out * heads_out, axis=2, keepdims=True)
        normed_part = (heads_out * lax.rsqrt(mean_sq + eps) * out_gain).astype(jnp.bfloat16)
        rows = state[2].shape[1]
        return normed_part.transpose(1, 0, 2).reshape(rows, heads_here * value_dim)

    init_state = tuple((initial(group[1].shape[0]) for group in query_groups))
    key_cols = key_rows.T
    value_cols = value_rows.T
    key_piece, value_piece = sent_together((key_cols, value_cols), "ep", 1, 0)
    shard_count = key_piece.shape[1] // seg_rows
    stride = max(1, 2048 // seg_rows)
    while shard_count % stride:
        stride -= 1
    fold_block_rows = stride * seg_rows
    turns = shard_count // stride

    def advance(step_num, states):
        key_start = step_num * fold_block_rows
        key_blk = lax.dynamic_slice_in_dim(
            key_piece, step_num * fold_block_rows, fold_block_rows, 1
        ).reshape(heads_here, 2, query_dim, fold_block_rows)
        value_blk = lax.dynamic_slice_in_dim(
            value_piece, step_num * fold_block_rows, fold_block_rows, 1
        ).reshape(heads_here, value_dim, fold_block_rows)
        updated = []
        for group, state in zip(query_groups, states):
            query_part, query_pos = group

            def apply_block(inside, query_part=query_part, query_pos=query_pos):
                return key_block(inside, query_part, query_pos, key_blk, value_blk, key_start)

            updated.append(
                lax.cond(key_start <= query_pos[-1], apply_block, lambda inside: inside, state)
            )
        return tuple(updated)

    folded = lax.fori_loop(0, turns, advance, init_state)
    late_heads = finish(folded[1])
    for bit in range(bit_count):
        late_heads = from_partner(late_heads, "ep", bit)
    normed_heads = jnp.concatenate([finish(folded[0]), late_heads], axis=0)
    tok_wide = tokens.astype(jnp.float32)
    normed = (
        tok_wide * lax.rsqrt(jnp.mean(tok_wide * tok_wide, axis=1, keepdims=True) + eps) * norm_gain
    ).astype(jnp.bfloat16)
    target = (group_ids[:, None] * group_size + inner_ids).reshape(-1)
    labels = jnp.arange(experts, dtype=jnp.int32)
    onehot = (target[:, None] == labels[None, :]).astype(jnp.int32)
    slot_rank = jnp.sum((jnp.cumsum(onehot, axis=0) - 1) * onehot, axis=1)
    slot_of = target * capacity + slot_rank
    slot_ids = jnp.arange(experts * capacity, dtype=jnp.int32)
    placing = jnp.any(
        (slot_of[:, None] == slot_ids[None, :]).reshape(tok_dev, topk_count, experts * capacity),
        axis=1,
    ).astype(jnp.bfloat16)
    outgoing = jnp.einsum("ts,td->sd", placing, normed, preferred_element_type=jnp.float32).astype(
        jnp.bfloat16
    )
    arrived = lax.all_to_all(outgoing, "ep", split_axis=0, concat_axis=0, tiled=True)
    arrived_rows = arrived.shape[0]
    gate_local = gate_weight[0]
    up_local = up_weight[0]
    down_local = down_weight[0]
    shard_rows = lax.all_gather(arrived, "tp", axis=0, tiled=True)
    gate_pre = jnp.dot(shard_rows, gate_local, preferred_element_type=jnp.float32)
    up_pre = jnp.dot(shard_rows, up_local, preferred_element_type=jnp.float32)
    hidden = (jax.nn.silu(gate_pre) * up_pre).astype(jnp.bfloat16)
    block_rows = tok_dev + arrived_rows
    row_count = lax.axis_size("tp") * block_rows
    repeats = row_count // block_rows
    mix_term = jnp.dot(normed_heads, out_weight, preferred_element_type=jnp.float32)
    expert_term = jnp.dot(hidden, down_local, preferred_element_type=jnp.float32)
    joined = jnp.concatenate(
        [
            mix_term.reshape(repeats, tok_dev, model_width),
            expert_term.reshape(repeats, arrived_rows, model_width),
        ],
        axis=1,
    )
    summed = lax.psum_scatter(
        joined.reshape(row_count, model_width).astype(jnp.bfloat16),
        "tp",
        scatter_dimension=0,
        tiled=True,
    ).astype(jnp.float32)
    attended = summed[:tok_dev].astype(jnp.bfloat16)
    results = summed[tok_dev:].astype(jnp.bfloat16)
    returned = lax.all_to_all(results, "ep", split_axis=0, concat_axis=0, tiled=True)
    picked = returned[slot_of].reshape(tok_dev, topk_count, model_width)
    combined = jnp.sum(picked.astype(jnp.float32) * route_weights[:, :, None], axis=1).astype(
        jnp.bfloat16
    )
    return (attended, combined)


def solution(mesh):
    in_specs = (
        P("ep", "tp"),
        P("ep", "tp"),
        P("ep", "tp"),
        P("tp"),
        P(),
        P("tp", None),
        P(("ep", "tp"), None),
        P(),
        P(("ep", "tp")),
        P(("ep", "tp"), None),
        P(("ep", "tp"), None),
        P("ep", None, "tp"),
        P("ep", None, "tp"),
        P("ep", "tp", None),
    )
    out_specs = (P(("ep", "tp"), None), P(("ep", "tp"), None))
    return jax.shard_map(body, mesh=mesh, in_specs=in_specs, out_specs=out_specs, check_vma=False)
```

profile of v0, /device:TPU:1, one launch (start us, length us, event | category | flops | bytes accessed | tf_op | source)
XLA Modules:
  0.0 413.3 jit_solution(1496006158266660823)
XLA Ops:
  18.7 9.6 %all-to-all-start = ((bf16[32,10,2048]{2,1,0:T(8,128)(2,1)}), bf16[32,10,2048]{2,1,0:T(8,128)(2,1)S(1)}, u32[]{:S(2)}, u32[]{:S(2)}) async-start(bf16[32,10,2048]{2,1,0:T(8,128)(2,1)} %all_to_all.16), calls=%async_computation | async-start | bytes 4194304 | tf_op jit(solution)/shard_map/all_to_all | solution.py:171
  32.2 29.1 %collective-permute-done.1 = bf16[256,256]{0,1:T(8,128)(2,1)S(1)} collective-permute-done((bf16[256,256]{0,1:T(8,128)(2,1)S(1)}, bf16[256,256]{0,1:T(8,128)(2,1)S(1)}, u32[]{:S(2)}, u32[]{:S(2)}) %collective-permute-start.1) | collective-permute-done | bytes 131104 | tf_op jit(solution)/shard_map/ppermute | solution.py:20
  69.3 3.1 collective-permute-done.3
  73.8 7.7 %collective-permute-done.4 = bf16[256,256]{0,1:T(8,128)(2,1)S(1)} collective-permute-done((bf16[256,256]{0,1:T(8,128)(2,1)S(1)}, bf16[256,256]{0,1:T(8,128)(2,1)S(1)}, u32[]{:S(2)}, u32[]{:S(2)}) %collective-permute-start.4) | collective-permute-done | bytes 131104 | tf_op jit(solution)/shard_map/ppermute | solution.py:20
  81.6 37.8 %all-gather.3.cloned.1.call-done = bf16[512,16384]{1,0:T(8,128)(2,1)} async-done(((bf16[512,512]{1,0:T(8,128)(2,1)}), bf16[512,16384]{1,0:T(8,128)(2,1)}) %all-gather.3.cloned.1.call-update) | async-done | bytes 16777232 | tf_op jit(solution)/shard_map/all_gather | solution.py:26
  119.4 11.8 %fusion.80 = (bf16[256,16384]{1,0:T(8,128)(2,1)}, bf16[256,16384]{1,0:T(8,128)(2,1)}) fusion(bf16[512,16384]{1,0:T(8,128)(2,1)} %all-gather.3.cloned.1.call-done), kind=kLoop, calls=%fused_computation.125 | loop fusion | bytes 33554432 | tf_op jit(solution)/shard_map/split | solution.py:27
  134.1 114.1 %while.35 = (s32[]{:T(128)}, f32[2,256]{1,0:T(2,128)S(1)}, f32[2,256]{1,0:T(2,128)S(1)}, f32[2,256,128]{2,1,0:T(8,128)}, f32[2,256]{1,0:T(2,128)S(1)}, /*index=5...) while((s32[]{:T(128)}, f32[2,256]{1,0:T(2,128)S(1)}, ...), condition=%wide.region_13.14_spmd, body=%wide.region_0.13_spmd.sunk | while | flops 1666719744 | bytes 85363600 | solution.py:149
  137.3 8.9 %conditional.5 = ((f32[2,256]{1,0:T(2,128)S(1)}, f32[2,256]{1,0:T(2,128)S(1)}, f32[2,256,128]{2,1,0:T(8,128)}, f32[2,256]{1,0:T(2,128)S(1)}, f32[2,256]{1,0:T(2,128)S(1)}, /*index=5*/f32[2,256,128]{2,1,0:T(8,128)})) conditional(s32[]{:T(128)} %convert_element_type.113, (f32[2,256]{1,0:T(2,128)S(1)}, f32[2,256]{1,0:T(2,128)S(1)}, ...), branch_computations={%region_7.7_spmd, %region_8.12_spmd} | conditional | flops 833359872 | bytes 40584364 | solution.py:145
  147.4 8.9 %conditional.4 = ((f32[2,256]{1,0:T(2,128)S(1)}, f32[2,256]{1,0:T(2,128)S(1)}, f32[2,256,128]{2,1,0:T(8,128)}, f32[2,256]{1,0:T(2,128)S(1)}, f32[2,256]{1,0:T(2,128)S(1)}, /*index=5*/f32[2,256,128]{2,1,0:T(8,128)})) conditional(s32[]{:T(128)} %convert_element_type.112, (f32[2,256]{1,0:T(2,128)S(1)}, f32[2,256]{1,0:T(2,128)S(1)}, ...), branch_computations={%region_1.0_spmd, %region_2.6_spmd} | conditional | flops 833359872 | bytes 40584364 | solution.py:145
  159.2 8.9 %conditional.5 = ((f32[2,256]{1,0:T(2,128)S(1)}, f32[2,256]{1,0:T(2,128)S(1)}, f32[2,256,128]{2,1,0:T(8,128)}, f32[2,256]{1,0:T(2,128)S(1)}, f32[2,256]{1,0:T(2,128)S(1)}, /*index=5*/f32[2,256,128]{2,1,0:T(8,128)})) conditional(s32[]{:T(128)} %convert_element_type.113, (f32[2,256]{1,0:T(2,128)S(1)}, f32[2,256]{1,0:T(2,128)S(1)}, ...), branch_computations={%region_7.7_spmd, %region_8.12_spmd} | conditional | flops 833359872 | bytes 40584364 | solution.py:145
  172.4 8.9 %conditional.5 = ((f32[2,256]{1,0:T(2,128)S(1)}, f32[2,256]{1,0:T(2,128)S(1)}, f32[2,256,128]{2,1,0:T(8,128)}, f32[2,256]{1,0:T(2,128)S(1)}, f32[2,256]{1,0:T(2,128)S(1)}, /*index=5*/f32[2,256,128]{2,1,0:T(8,128)})) conditional(s32[]{:T(128)} %convert_element_type.113, (f32[2,256]{1,0:T(2,128)S(1)}, f32[2,256]{1,0:T(2,128)S(1)}, ...), branch_computations={%region_7.7_spmd, %region_8.12_spmd} | conditional | flops 833359872 | bytes 40584364 | solution.py:145
  185.5 8.9 %conditional.5 = ((f32[2,256]{1,0:T(2,128)S(1)}, f32[2,256]{1,0:T(2,128)S(1)}, f32[2,256,128]{2,1,0:T(8,128)}, f32[2,256]{1,0:T(2,128)S(1)}, f32[2,256]{1,0:T(2,128)S(1)}, /*index=5*/f32[2,256,128]{2,1,0:T(8,128)})) conditional(s32[]{:T(128)} %convert_element_type.113, (f32[2,256]{1,0:T(2,128)S(1)}, f32[2,256]{1,0:T(2,128)S(1)}, ...), branch_computations={%region_7.7_spmd, %region_8.12_spmd} | conditional | flops 833359872 | bytes 40584364 | solution.py:145
  198.6 8.9 %conditional.5 = ((f32[2,256]{1,0:T(2,128)S(1)}, f32[2,256]{1,0:T(2,128)S(1)}, f32[2,256,128]{2,1,0:T(8,128)}, f32[2,256]{1,0:T(2,128)S(1)}, f32[2,256]{1,0:T(2,128)S(1)}, /*index=5*/f32[2,256,128]{2,1,0:T(8,128)})) conditional(s32[]{:T(128)} %convert_element_type.113, (f32[2,256]{1,0:T(2,128)S(1)}, f32[2,256]{1,0:T(2,128)S(1)}, ...), branch_computations={%region_7.7_spmd, %region_8.12_spmd} | conditional | flops 833359872 | bytes 40584364 | solution.py:145
  211.7 8.9 %conditional.5 = ((f32[2,256]{1,0:T(2,128)S(1)}, f32[2,256]{1,0:T(2,128)S(1)}, f32[2,256,128]{2,1,0:T(8,128)}, f32[2,256]{1,0:T(2,128)S(1)}, f32[2,256]{1,0:T(2,128)S(1)}, /*index=5*/f32[2,256,128]{2,1,0:T(8,128)})) conditional(s32[]{:T(128)} %convert_element_type.113, (f32[2,256]{1,0:T(2,128)S(1)}, f32[2,256]{1,0:T(2,128)S(1)}, ...), branch_computations={%region_7.7_spmd, %region_8.12_spmd} | conditional | flops 833359872 | bytes 40584364 | solution.py:145
  224.8 8.9 %conditional.5 = ((f32[2,256]{1,0:T(2,128)S(1)}, f32[2,256]{1,0:T(2,128)S(1)}, f32[2,256,128]{2,1,0:T(8,128)}, f32[2,256]{1,0:T(2,128)S(1)}, f32[2,256]{1,0:T(2,128)S(1)}, /*index=5*/f32[2,256,128]{2,1,0:T(8,128)})) conditional(s32[]{:T(128)} %convert_element_type.113, (f32[2,256]{1,0:T(2,128)S(1)}, f32[2,256]{1,0:T(2,128)S(1)}, ...), branch_computations={%region_7.7_spmd, %region_8.12_spmd} | conditional | flops 833359872 | bytes 40584364 | solution.py:145
  237.9 8.9 %conditional.5 = ((f32[2,256]{1,0:T(2,128)S(1)}, f32[2,256]{1,0:T(2,128)S(1)}, f32[2,256,128]{2,1,0:T(8,128)}, f32[2,256]{1,0:T(2,128)S(1)}, f32[2,256]{1,0:T(2,128)S(1)}, /*index=5*/f32[2,256,128]{2,1,0:T(8,128)})) conditional(s32[]{:T(128)} %convert_element_type.113, (f32[2,256]{1,0:T(2,128)S(1)}, f32[2,256]{1,0:T(2,128)S(1)}, ...), branch_computations={%region_7.7_spmd, %region_8.12_spmd} | conditional | flops 833359872 | bytes 40584364 | solution.py:145
  254.5 4.8 %collective-permute-done.6 = bf16[256,256]{0,1:T(8,128)(2,1)S(1)} collective-permute-done((bf16[256,256]{0,1:T(8,128)(2,1)S(1)}, bf16[256,256]{0,1:T(8,128)(2,1)S(1)}, u32[]{:S(2)}, u32[]{:S(2)}) %collective-permute-start.6) | collective-permute-done | bytes 131104 | tf_op jit(solution)/shard_map/ppermute | solution.py:20
  259.6 4.2 %fusion.66 = f32[1280,256]{1,0:T(8,128)S(1)} fusion(bf16[1280,2048]{1,0:T(8,128)(2,1)} %all-gather.5.cloned.1.call-done, bf16[1,2048,256]{2,1,0:T(8,128)(2,1)S(1)} %copy-done.18), kind=kOutput, calls=%fused_computation.89 | convolution fusion | flops 1342177280 | bytes 7602176 | tf_op jit(solution)/shard_map/dot_general | solution.py:177
  266.0 2.9 fusion.60
  276.5 5.5 %pad_maximum_fusion = bf16[4,448,2048]{2,1,0:T(8,128)(2,1)} fusion(bf16[4,320,2048]{2,1,0:T(8,128)(2,1)S(1)} %convolution_convert_fusion, bf16[4,128,2048]{2,1,0:T(8,128)(2,1)} %bitcast.102), kind=kLoop, calls=%fused_computation.75 | loop fusion | flops 14680064 | bytes 14680064 | tf_op jit(solution)/shard_map/concatenate | solution.py:185
  282.0 74.6 %reduce-scatter.2.cloned.1.call-done = bf16[448,2048]{1,0:T(8,128)(2,1)} async-done(((bf16[1792,2048]{1,0:T(8,128)(2,1)}), bf16[448,2048]{1,0:T(8,128)(2,1)}) %reduce-scatter.2.cloned.1.call-update) | async-done | bytes 1835024 | tf_op jit(solution)/shard_map/reduce_scatter | solution.py:192
  359.6 7.8 %all-to-all-start.1 = ((bf16[32,10,2048]{2,1,0:T(8,128)(2,1)}), bf16[32,10,2048]{2,1,0:T(8,128)(2,1)}, u32[]{:S(2)}, u32[]{:S(2)}) async-start(bf16[32,10,2048]{2,1,0:T(8,128)(2,1)} %all_to_all.19), calls=%async_computation.2 | async-start | bytes 4194304 | tf_op jit(solution)/shard_map/all_to_all | solution.py:200
  369.6 26.0 %all-to-all-done.1 = bf16[32,10,2048]{2,1,0:T(8,128)(2,1)} async-done(((bf16[32,10,2048]{2,1,0:T(8,128)(2,1)}), bf16[32,10,2048]{2,1,0:T(8,128)(2,1)}, u32[]{:S(2)}, u32[]{:S(2)}) %all-to-all-start.1) | async-done | bytes 1310752 | tf_op jit(solution)/shard_map/all_to_all | solution.py:200
  402.9 3.9 multiply_reduce_fusion
  (318 shorter events, 158.1 us)
Async XLA Ops:
  7.2 263.3 %copy-start = (bf16[1,256,2048]{2,1,0:T(8,128)(2,1)S(1)}, bf16[1,256,2048]{2,1,0:T(8,128)(2,1)}, u32[]{:S(2)}) copy-start(bf16[1,256,2048]{2,1,0:T(8,128)(2,1)} %param.33) | copy-start | bytes 3145732
  7.2 8.7 %copy-start.1 = (bf16[128,2048]{1,0:T(8,128)(2,1)S(1)}, bf16[128,2048]{1,0:T(8,128)(2,1)}, u32[]{:S(2)}) copy-start(bf16[128,2048]{1,0:T(8,128)(2,1)} %param.26) | copy-start | bytes 1572868
  7.2 112.2 %all-gather.3.cloned.1.call-start = ((), (), s32[]{:S(2)}) async-start(), calls=%async_computation.3 | async-start | bytes 17301504 | tf_op jit(solution)/shard_map/all_gather | solution.py:26
  18.7 49.3 %all-to-all-start = ((bf16[32,10,2048]{2,1,0:T(8,128)(2,1)}), bf16[32,10,2048]{2,1,0:T(8,128)(2,1)S(1)}, u32[]{:S(2)}, u32[]{:S(2)}) async-start(bf16[32,10,2048]{2,1,0:T(8,128)(2,1)} %all_to_all.16), calls=%async_computation | async-start | bytes 4194304 | tf_op jit(solution)/shard_map/all_to_all | solution.py:171
  28.3 231.3 %all-gather.5.cloned.1.call-start = ((), (), s32[]{:S(2)}) async-start(), calls=%async_computation.4 | async-start | bytes 6553600 | tf_op jit(solution)/shard_map/all_gather | solution.py:176
  29.4 1.4 collective-permute-start
  30.9 30.5 %collective-permute-start.1 = (bf16[256,256]{0,1:T(8,128)(2,1)S(1)}, bf16[256,256]{0,1:T(8,128)(2,1)S(1)}, u32[]{:S(2)}, u32[]{:S(2)}) collective-permute-start(bf16[256,256]{0,1:T(8,128)(2,1)S(1)} %collective-permute-done), channel_id=1, source_target_pairs={{0,8},{8,0},{4,12},{12,4},{16,24},{24,16},{20,28},{28,20},{32,40},... | collective-permute-start | bytes 393224 | tf_op jit(solution)/shard_map/ppermute | solution.py:20
  61.4 5.3 %collective-permute-start.2 = (bf16[256,256]{0,1:T(8,128)(2,1)S(1)}, bf16[256,256]{0,1:T(8,128)(2,1)S(1)}, u32[]{:S(2)}, u32[]{:S(2)}) collective-permute-start(bf16[256,256]{0,1:T(8,128)(2,1)S(1)} %collective-permute-done.1), channel_id=1, source_target_pairs={{0,16},{16,0},{4,20},{20,4},{8,24},{24,8},{12,28},{28,12},{32,48},... | collective-permute-start | bytes 393224 | tf_op jit(solution)/shard_map/ppermute | solution.py:20
  66.7 5.7 %collective-permute-start.3 = (bf16[256,256]{0,1:T(8,128)(2,1)S(1)}, bf16[256,256]{0,1:T(8,128)(2,1)S(1)}, u32[]{:S(2)}, u32[]{:S(2)}) collective-permute-start(bf16[256,256]{0,1:T(8,128)(2,1)S(1)} %collective-permute-done.2), channel_id=1, source_target_pairs={{0,32},{32,0},{4,36},{36,4},{8,40},{40,8},{12,44},{44,12},{16,48},... | collective-permute-start | bytes 393224 | tf_op jit(solution)/shard_map/ppermute | solution.py:20
  69.3 287.3 %reduce-scatter.2.cloned.1.call-start = ((), (), s32[]{:S(2)}) async-start(), calls=%async_computation.5 | async-start | bytes 9175040 | tf_op jit(solution)/shard_map/reduce_scatter | solution.py:192
  72.4 9.2 %collective-permute-start.4 = (bf16[256,256]{0,1:T(8,128)(2,1)S(1)}, bf16[256,256]{0,1:T(8,128)(2,1)S(1)}, u32[]{:S(2)}, u32[]{:S(2)}) collective-permute-start(bf16[256,256]{0,1:T(8,128)(2,1)S(1)} %collective-permute-done.3), channel_id=1, source_target_pairs={{0,64},{64,0},{4,68},{68,4},{8,72},{72,8},{12,76},{76,12},{16,80},... | collective-permute-start | bytes 393224 | tf_op jit(solution)/shard_map/ppermute | solution.py:20
  134.1 118.6 %copy-start.15 = (f32[2]{0:T(128)S(1)}, f32[2]{0:T(128)}, u32[]{:S(2)}) copy-start(f32[2]{0:T(128)} %param.23) | copy-start | bytes 28
  134.1 118.9 %copy-start.16 = (f32[128]{0:T(128)S(1)}, f32[128]{0:T(128)}, u32[]{:S(2)}) copy-start(f32[128]{0:T(128)} %param.24) | copy-start | bytes 1540
  248.3 11.3 %copy-start.18 = (bf16[1,2048,256]{2,1,0:T(8,128)(2,1)S(1)}, bf16[1,2048,256]{2,1,0:T(8,128)(2,1)}, u32[]{:S(2)}) copy-start(bf16[1,2048,256]{2,1,0:T(8,128)(2,1)} %param.31) | copy-start | bytes 3145732
  253.1 1.4 collective-permute-start.5
  254.5 4.8 %collective-permute-start.6 = (bf16[256,256]{0,1:T(8,128)(2,1)S(1)}, bf16[256,256]{0,1:T(8,128)(2,1)S(1)}, u32[]{:S(2)}, u32[]{:S(2)}) collective-permute-start(bf16[256,256]{0,1:T(8,128)(2,1)S(1)} %collective-permute-done.5), channel_id=1, source_target_pairs={{0,8},{8,0},{4,12},{12,4},{16,24},{24,16},{20,28},{28,20},{32,40},... | collective-permute-start | bytes 393224 | tf_op jit(solution)/shard_map/ppermute | solution.py:20
  259.4 5.3 %collective-permute-start.7 = (bf16[256,256]{0,1:T(8,128)(2,1)S(1)}, bf16[256,256]{0,1:T(8,128)(2,1)S(1)}, u32[]{:S(2)}, u32[]{:S(2)}) collective-permute-start(bf16[256,256]{0,1:T(8,128)(2,1)S(1)} %collective-permute-done.6), channel_id=1, source_target_pairs={{0,16},{16,0},{4,20},{20,4},{8,24},{24,8},{12,28},{28,12},{32,48},... | collective-permute-start | bytes 393224 | tf_op jit(solution)/shard_map/ppermute | solution.py:20
  259.6 6.4 %copy-start.17 = (bf16[1280,2048]{1,0:T(8,128)(2,1)S(1)}, bf16[1280,2048]{1,0:T(8,128)(2,1)}, u32[]{:S(2)}) copy-start(bf16[1280,2048]{1,0:T(8,128)(2,1)} %all-gather.5.cloned.1.call-done) | copy-start | bytes 15728644
  264.7 4.3 %collective-permute-start.8 = (bf16[256,256]{0,1:T(8,128)(2,1)S(1)}, bf16[256,256]{0,1:T(8,128)(2,1)S(1)}, u32[]{:S(2)}, u32[]{:S(2)}) collective-permute-start(bf16[256,256]{0,1:T(8,128)(2,1)S(1)} %collective-permute-done.7), channel_id=1, source_target_pairs={{0,32},{32,0},{4,36},{36,4},{8,40},{40,8},{12,44},{44,12},{16,48},... | collective-permute-start | bytes 393224 | tf_op jit(solution)/shard_map/ppermute | solution.py:20
  269.0 5.4 %collective-permute-start.9 = (bf16[256,256]{0,1:T(8,128)(2,1)S(1)}, bf16[256,256]{0,1:T(8,128)(2,1)S(1)}, u32[]{:S(2)}, u32[]{:S(2)}) collective-permute-start(bf16[256,256]{0,1:T(8,128)(2,1)S(1)} %collective-permute-done.8), channel_id=1, source_target_pairs={{0,64},{64,0},{4,68},{68,4},{8,72},{72,8},{12,76},{76,12},{16,80},... | collective-permute-start | bytes 393224 | tf_op jit(solution)/shard_map/ppermute | solution.py:20
  358.0 9.4 %copy-start.11 = (s32[128,2]{1,0:T(8,128)S(1)}, s32[128,2]{1,0:T(8,128)}, u32[]{:S(2)}) copy-start(s32[128,2]{1,0:T(8,128)} %get-tuple-element.583) | copy-start | bytes 3076
  358.0 9.5 %copy-start.14 = (f32[128,2]{0,1:T(2,128)S(1)}, f32[128,2]{0,1:T(2,128)}, u32[]{:S(2)}) copy-start(f32[128,2]{0,1:T(2,128)} %param.30) | copy-start | bytes 3076
  358.0 9.7 %copy-start.13 = (s32[256]{0:T(256)S(1)}, s32[256]{0:T(256)}, u32[]{:S(2)}) copy-start(s32[256]{0:T(256)} %copy-done.12) | copy-start | bytes 3076
  359.6 36.1 %all-to-all-start.1 = ((bf16[32,10,2048]{2,1,0:T(8,128)(2,1)}), bf16[32,10,2048]{2,1,0:T(8,128)(2,1)}, u32[]{:S(2)}, u32[]{:S(2)}) async-start(bf16[32,10,2048]{2,1,0:T(8,128)(2,1)} %all_to_all.19), calls=%async_computation.2 | async-start | bytes 4194304 | tf_op jit(solution)/shard_map/all_to_all | solution.py:200
  (38 other events, 60.5 us)
Sparse Core Ops, SparseCore 0:
  10.8 108.5 all-gather.2
  121.0 55.4 all-gather.4
  282.1 74.4 reduce-scatter.1
where the time goes:
time: 415 us; the launch traced here: 413 us
  waiting for transfers between devices  192 us (46%)
  local copies, waits for them, and re-layouts  69.4 us (17%)
  matrix products  58.7 us (14%)
  other arithmetic  39.7 us (10%)
  starting transfers between devices  27.5 us (7%)
  between operations  14.2 us (3%)
  loops' own time  12.2 us (3%)
    reduce_scatter x1, waiting for transfers between devices, body(): lax.psum_scatter(joined.reshape(row_count, model_width).astype(jnp.bfloat...  74.6 us
    ppermute x10, waiting for transfers between devices, from_partner(): return lax.ppermute(block, axis, route)  53.1 us
    all_gather x1, waiting for transfers between devices, sent_together(): out = lax.all_gather(both, axis, axis=dim, tiled=True)  37.8 us
    all_to_all x1, waiting for transfers between devices, body(): lax.all_to_all(results, 'ep', split_axis=0, concat_axis=0, tiled=True)  26 us
    dot_general x18, matrix products, one_map(): jnp.einsum('hqk,hdk->hqd', exps.astype(jnp.bfloat16), value_blk, preferre...  25.2 us
    reduce_sum x9, other arithmetic, one_map(): total_new = total_old * fade + jnp.sum(exps, axis=2)  22.2 us
    dot_general x18, matrix products, one_map(): jnp.einsum('hqd,hdk->hqk', query_map, key_map, preferred_element_type=jnp...  21.4 us
    dynamic_slice x8, local copies, waits for them, and re-layouts, advance(): lax.dynamic_slice_in_dim(value_piece, step_num * fold_block_rows, fold_bl...  13.5 us
  transfers between devices with their start and end apart: 15, of which 12 were waited for; matrix products, arithmetic and copies ran while one was open for 32% of the time, Pallas kernels for 0%

commit v1 on v0

v1 whole, which is shorter than its diff:
```python
import functools
import math

import jax
import jax.numpy as jnp
from jax import lax
from jax.experimental import pallas as pl
from jax.experimental.pallas import tpu as pltpu
from jax.sharding import PartitionSpec as P

GROUPS = 4
SIDE = 4
CHIPS = 16
MESH = pl.DeviceIdType.MESH

eps = 1e-06
neg_big = -1e30
f32 = jnp.float32
bf16 = jnp.bfloat16


def wrap(v):
    return lax.rem(v + SIDE, SIDE)


def attention_kernel(
    q_ref,
    k_ref,
    v_ref,
    lam_ref,
    gain_ref,
    ow_ref,
    out_ref,
    kv,
    give,
    qb,
    qt,
    acc,
    top,
    tot,
    ow,
    heads,
    outgoing,
    pre_send,
    pre_recv,
    here,
    kv_send,
    kv_recv,
    ow_send,
    ow_recv,
    head_send,
    head_recv,
):
    ep = lax.axis_index("ep")
    x = lax.axis_index("tp")
    chip = ep // 2
    core = lax.rem(ep, 2)
    mate = 1 - core
    mirror = CHIPS - 1 - chip
    at_z, at_y = chip // SIDE, lax.rem(chip, SIDE)
    right, left, far = wrap(x + 1), wrap(x - 1), wrap(x + 2)
    scale = (64 ** (-0.5)) * math.log2(math.e)

    def remote(src, dst, send, recv, to):
        return pltpu.make_async_remote_copy(
            src_ref=src, dst_ref=dst, send_sem=send, recv_sem=recv, device_id=to, device_id_type=MESH
        )

    def cols(head):
        return pl.ds(pl.multiple_of(head * 128, 128), 128)

    def chip_at(dz, dy):
        return wrap(at_z + dz) * SIDE + wrap(at_y + dy)

    partner = (2 * chip + mate, x)

    keep_q = pltpu.make_async_copy(q_ref.at[:, cols(0)], qb.at[0], here.at[0])
    give_q = remote(q_ref.at[:, cols(1)], qb.at[0], pre_send.at[1], pre_recv.at[1], partner)
    far_q = [
        remote(q_ref.at[:, cols(h)], qb.at[1], pre_send.at[1 + h], pre_recv.at[2], (2 * mirror + h, x))
        for h in range(2)
    ]

    @pl.when(core == 0)
    def _():
        keep_q.start()
        give_q.start()

    @pl.when(core == 1)
    def _():
        far_q[0].start()
        far_q[1].start()

    def lay_out(head, put):
        for p in range(2):
            put(p, pl.ds(0, 256), k_ref[pl.ds(p * 256, 256), cols(head)])
            for n in range(2):
                block = v_ref[pl.ds(p * 256 + n * 128, 128), cols(head)].astype(f32)
                put(p, pl.ds(256 + n * 128, 128), block.T.astype(bf16))

    def put_give(p, rows, value):
        give[p, rows, :] = value

    def put_own(p, rows, value):
        kv[chip, 2 * core + p, rows, :] = value

    lay_out(mate, put_give)
    half_of = kv.at[chip, pl.ds(2 * core, 2)]
    give_kv = remote(give, half_of, pre_send.at[0], pre_recv.at[0], partner)
    give_kv.start()
    lay_out(core, put_own)

    def step_to(axis, sign):
        return chip_at(sign, 0) if axis == 0 else chip_at(0, sign)

    def moved(place, axis, by):
        dz, dy = place
        return (dz + by, dy) if axis == 0 else (dz, dy + by)

    def spread(half, n, place, axis):
        def copy(slot):
            sign = 1 if slot % 2 == 0 else -1
            if slot < 2:
                j, part = chip_at(*place), pl.ds(2 * half, 2)
            else:
                j, part = chip_at(*moved(place, axis, -sign)), pl.ds(2 * half + slot - 2, 1)
            at = kv.at[j, part]
            return remote(
                at, at, kv_send.at[half, n, slot], kv_recv.at[half, n, slot], (2 * step_to(axis, sign) + core, x)
            )

        return [copy(slot) for slot in range(4)]

    first_axis = (1, 0)
    phase = [[None] * 5, [None] * 5]
    for half in range(2):
        one, two = first_axis[half], 1 - first_axis[half]
        phase[half][0] = spread(half, 0, (0, 0), one)
        for n, by in enumerate((0, -1, 1, 2)):
            phase[half][1 + n] = spread(half, 1 + n, moved((0, 0), one, by), two)
    sent = [c for half in range(2) for group in phase[half] for c in group]

    give_kv.wait_recv()
    for n in range(2):
        for half in range(2):
            phase[half][n][0].start()
            phase[half][n][1].start()

    keep_ow = pltpu.make_async_copy(ow_ref, ow.at[pl.ds(2 * x, 2)], here.at[1])
    keep_ow.start()

    def ow_rows(at_x, c):
        return ow.at[2 * at_x + c]

    ow_right = remote(ow_ref.at[core], ow_rows(x, core), ow_send.at[0], ow_recv.at[0], (ep, right))
    ow_left = remote(ow_ref.at[core], ow_rows(x, core), ow_send.at[1], ow_recv.at[1], (ep, left))
    ow_right.start()
    ow_left.start()
    top_half, low_half = pl.ds(0, 64), pl.ds(64, 64)
    on_right = remote(
        ow_rows(left, core).at[top_half],
        ow_rows(left, core).at[top_half],
        ow_send.at[2],
        ow_recv.at[2],
        (ep, right),
    )
    on_left = remote(
        ow_rows(right, core).at[low_half],
        ow_rows(right, core).at[low_half],
        ow_send.at[3],
        ow_recv.at[3],
        (ep, left),
    )

    def across(n, at_x):
        return remote(ow_rows(at_x, core), ow_rows(at_x, core), ow_send.at[4 + n], ow_recv.at[4 + n], partner)

    across_copies = [across(0, left), across(1, right), across(2, far)]

    @pl.when(core == 0)
    def _():
        keep_q.wait()

    @pl.when(core == 1)
    def _():
        give_q.wait_recv()

    far_q[0].wait_recv()

    depth = lax.broadcasted_iota(jnp.int32, (128, 128), 0)
    for b in range(2):
        for n in range(4):
            flipped = qb[b, pl.ds(n * 128, 128), :].astype(f32).T
            at = pl.ds(n * 128, 128)
            qt[b, 0, :, at] = jnp.where(depth < 64, flipped, 0.0).astype(bf16)
            qt[b, 1, :, at] = jnp.where(depth < 64, 0.0, flipped).astype(bf16)
    top[...] = jnp.full(top.shape, neg_big, f32)
    tot[...] = jnp.zeros(tot.shape, f32)
    acc[...] = jnp.zeros(acc.shape, f32)

    def unit(b, j, half, masked):
        for n in range(2):
            at = pl.ds(n * 256, 256)
            for m in range(2):
                q = qt[b, m, :, at]
                scores = []
                for p in range(2):
                    keys = kv[j, 2 * half + p, 0:256, :]
                    part = jnp.dot(keys, q, preferred_element_type=f32)
                    if masked:
                        key = lax.broadcasted_iota(jnp.int32, (256, 256), 0) + p * 256
                        row = lax.broadcasted_iota(jnp.int32, (256, 256), 1) + n * 256
                        part = jnp.where(key <= row, part, neg_big)
                    scores.append(part)
                old = top[b, m, :, at]
                new = old
                for part in scores:
                    new = jnp.maximum(new, jnp.max(part, axis=0, keepdims=True))
                top[b, m, :, at] = new
                fade = jnp.exp2((old - new) * scale)
                total = tot[b, m, :, at] * fade
                numer = acc[b, m, :, at] * fade
                for p in range(2):
                    exps = jnp.exp2((scores[p] - new) * scale)
                    total = total + jnp.sum(exps, axis=0, keepdims=True)
                    values = jnp.concatenate(
                        [kv[j, 2 * half + p, 256:384, :], kv[j, 2 * half + p, 384:512, :]], axis=1
                    )
                    numer = numer + jnp.dot(values, exps.astype(bf16), preferred_element_type=f32)
                tot[b, m, :, at] = total
                acc[b, m, :, at] = numer

    limits = (chip, mirror)

    def batch(items):
        def one(i, carry):
            b = lax.rem(i, 2)
            nth = i // 2
            j, half = items[0][0], jnp.int32(items[0][1])
            for k in range(1, len(items)):
                j = jnp.where(nth == k, items[k][0], j)
                half = jnp.where(nth == k, items[k][1], half)
            limit = jnp.where(b == 0, limits[0], limits[1])

            @pl.when(j < limit)
            def _():
                unit(b, j, half, False)

            return carry

        lax.fori_loop(0, 2 * len(items), one, 0)

    def arrivals(group_at, kinds):
        items = []
        for half in range(2):
            one, two = first_axis[half], 1 - first_axis[half]
            for n in group_at:
                if n == 0:
                    base, axis = (0, 0), one
                else:
                    base, axis = moved((0, 0), one, (0, -1, 1, 2)[n - 1]), two
                for by in kinds:
                    items.append((chip_at(*moved(base, axis, by)), half))
        return items

    def direct(group_at):
        for n in group_at:
            for half in range(2):
                for slot in range(2):
                    phase[half][n][slot].wait_recv()
                    phase[half][n][slot + 2].start()

    def relayed(group_at):
        for n in group_at:
            for half in range(2):
                for slot in range(2):
                    phase[half][n][slot + 2].wait_recv()

    def begin(group_at):
        for n in group_at:
            for half in range(2):
                phase[half][n][0].start()
                phase[half][n][1].start()

    unit(0, chip, 0, True)
    batch([(jnp.where(chip < mirror, chip, CHIPS), 0), (jnp.where(chip < mirror, chip, CHIPS), 1)])
    direct((0,))
    begin((2, 3))
    batch(arrivals((0,), (-1, 1)))
    relayed((0,))
    begin((4,))
    direct((1,))
    ow_right.wait_recv()
    on_right.start()
    across_copies[0].start()
    ow_left.wait_recv()
    on_left.start()
    across_copies[1].start()
    batch(arrivals((0,), (2,)) + arrivals((1,), (-1, 1)))
    direct((2, 3))
    batch(arrivals((2,), (-1, 1)) + arrivals((3,), (-1, 1)))
    relayed((1,))
    direct((4,))
    on_right.wait_recv()
    on_left.wait_recv()
    across_copies[2].start()
    batch(arrivals((1,), (2,)) + arrivals((4,), (-1, 1)))
    relayed((2, 3, 4))
    batch(arrivals((2,), (2,)) + arrivals((3,), (2,)) + arrivals((4,), (2,)))
    unit(1, mirror, 0, False)
    unit(1, mirror, 1, True)

    lam = lam_ref[core]

    def to_owner(b, n, dst):
        send = outgoing.at[b, pl.ds(n * 128, 128)]
        return remote(
            send, heads.at[2 * x + core], head_send.at[b, n], head_recv.at[2 * x + core], (dst, n)
        )

    def home(n):
        return jnp.logical_and(core == 0, x == n)

    for b in (1, 0):
        for n in range(4):
            at = pl.ds(n * 128, 128)
            head = acc[b, 0, :, at] / tot[b, 0, :, at] - lam * (acc[b, 1, :, at] / tot[b, 1, :, at])
            mean_sq = jnp.mean(head * head, axis=0, keepdims=True)
            normed = (head * lax.rsqrt(mean_sq + eps)).T * gain_ref[...]
            outgoing[b, at, :] = normed.astype(bf16)
        for n in range(4):
            if b == 0:

                @pl.when(jnp.logical_not(home(n)))
                def _(n=n):
                    to_owner(0, n, 2 * chip).start()

                @pl.when(home(n))
                def _(n=n):
                    heads[2 * x] = outgoing[0, n * 128 : (n + 1) * 128, :]

            else:
                to_owner(1, n, 2 * mirror + 1).start()

    keep_ow.wait()
    for c in across_copies:
        c.wait_recv()

    for hd in range(8):

        @pl.when(jnp.logical_or(core == 1, 2 * x != hd))
        def _(hd=hd):
            remote(heads.at[hd], heads.at[hd], head_send.at[0, 0], head_recv.at[hd], partner).wait_recv()

    def project(n, carry):
        at = pl.ds(pl.multiple_of(n * 512, 512), 512)
        total = jnp.zeros((128, 512), f32)
        for hd in range(8):
            total = total + jnp.dot(heads[hd], ow[hd, :, at], preferred_element_type=f32)
        out_ref[:, at] = total.astype(bf16)
        return carry

    lax.fori_loop(0, 4, project, 0)

    give_kv.wait_send()

    @pl.when(core == 0)
    def _():
        give_q.wait_send()

    @pl.when(core == 1)
    def _():
        far_q[0].wait_send()
        far_q[1].wait_send()

    for c in sent + [ow_right, ow_left, on_right, on_left] + across_copies:
        c.wait_send()
    for n in range(4):

        @pl.when(jnp.logical_not(home(n)))
        def _(n=n):
            to_owner(0, n, 2 * chip).wait_send()

        to_owner(1, n, 2 * mirror + 1).wait_send()


def attention(query_rows, key_rows, value_rows, lambdas, out_gain, out_weight):
    any_space = pl.BlockSpec(memory_space=pl.ANY)
    vmem = pl.BlockSpec(memory_space=pltpu.VMEM)
    width = out_weight.shape[1]
    dma = pltpu.SemaphoreType.DMA
    return pl.pallas_call(
        attention_kernel,
        out_shape=jax.ShapeDtypeStruct((128, width), bf16),
        in_specs=[any_space, vmem, vmem, pl.BlockSpec(memory_space=pltpu.SMEM), vmem, any_space],
        out_specs=vmem,
        scratch_shapes=[
            pltpu.VMEM((CHIPS, 4, 512, 128), bf16),
            pltpu.VMEM((2, 512, 128), bf16),
            pltpu.VMEM((2, 512, 128), bf16),
            pltpu.VMEM((2, 2, 128, 512), bf16),
            pltpu.VMEM((2, 2, 128, 512), f32),
            pltpu.VMEM((2, 2, 1, 512), f32),
            pltpu.VMEM((2, 2, 1, 512), f32),
            pltpu.VMEM((8, 128, width), bf16),
            pltpu.VMEM((8, 128, 128), bf16),
            pltpu.VMEM((2, 512, 128), bf16),
            dma((3,)),
            dma((3,)),
            dma((2,)),
            dma((2, 5, 4)),
            dma((2, 5, 4)),
            dma((7,)),
            dma((7,)),
            dma((2, 4)),
            dma((8,)),
        ],
        compiler_params=pltpu.CompilerParams(has_side_effects=True, vmem_limit_bytes=40 * 2**20),
        name="attention",
    )(
        query_rows,
        key_rows,
        value_rows,
        lambdas,
        out_gain.reshape(1, -1),
        out_weight.reshape(2, 128, width),
    )


def experts_part(
    tokens, norm_gain, group_ids, inner_ids, route_weights, gate_weight, up_weight, down_weight
):
    tok_dev = tokens.shape[0]
    model_width = tokens.shape[1]
    topk_count = inner_ids.shape[1]
    experts = lax.axis_size("ep")
    group_size = experts // GROUPS
    capacity = 5 * tok_dev * topk_count // (4 * experts)
    tok_wide = tokens.astype(f32)
    normed = (
        tok_wide * lax.rsqrt(jnp.mean(tok_wide * tok_wide, axis=1, keepdims=True) + eps) * norm_gain
    ).astype(bf16)
    target = (group_ids[:, None] * group_size + inner_ids).reshape(-1)
    labels = jnp.arange(experts, dtype=jnp.int32)
    onehot = (target[:, None] == labels[None, :]).astype(jnp.int32)
    slot_rank = jnp.sum((jnp.cumsum(onehot, axis=0) - 1) * onehot, axis=1)
    slot_of = target * capacity + slot_rank
    slot_ids = jnp.arange(experts * capacity, dtype=jnp.int32)
    placing = jnp.any(
        (slot_of[:, None] == slot_ids[None, :]).reshape(tok_dev, topk_count, experts * capacity),
        axis=1,
    ).astype(bf16)
    outgoing = jnp.einsum("ts,td->sd", placing, normed, preferred_element_type=f32).astype(bf16)
    arrived = lax.all_to_all(outgoing, "ep", split_axis=0, concat_axis=0, tiled=True)
    shard_rows = lax.all_gather(arrived, "tp", axis=0, tiled=True)
    gate_pre = jnp.dot(shard_rows, gate_weight[0], preferred_element_type=f32)
    up_pre = jnp.dot(shard_rows, up_weight[0], preferred_element_type=f32)
    hidden = (jax.nn.silu(gate_pre) * up_pre).astype(bf16)
    expert_term = jnp.dot(hidden, down_weight[0], preferred_element_type=f32).astype(bf16)
    results = lax.psum_scatter(expert_term, "tp", scatter_dimension=0, tiled=True)
    returned = lax.all_to_all(results, "ep", split_axis=0, concat_axis=0, tiled=True)
    picked = returned[slot_of].reshape(tok_dev, topk_count, model_width)
    return jnp.sum(picked.astype(f32) * route_weights[:, :, None], axis=1).astype(bf16)


def body(
    query_rows,
    key_rows,
    value_rows,
    lambdas,
    out_gain,
    out_weight,
    tokens,
    norm_gain,
    group_ids,
    inner_ids,
    route_weights,
    gate_weight,
    up_weight,
    down_weight,
):
    attended = attention(query_rows, key_rows, value_rows, lambdas, out_gain, out_weight)
    combined = experts_part(
        tokens, norm_gain, group_ids, inner_ids, route_weights, gate_weight, up_weight, down_weight
    )
    return (attended, combined)


def solution(mesh):
    in_specs = (
        P("ep", "tp"),
        P("ep", "tp"),
        P("ep", "tp"),
        P("tp"),
        P(),
        P("tp", None),
        P(("ep", "tp"), None),
        P(),
        P(("ep", "tp")),
        P(("ep", "tp"), None),
        P(("ep", "tp"), None),
        P("ep", None, "tp"),
        P("ep", None, "tp"),
        P("ep", "tp", None),
    )
    out_specs = (P(("ep", "tp"), None), P(("ep", "tp"), None))
    return jax.shard_map(body, mesh=mesh, in_specs=in_specs, out_specs=out_specs, check_vma=False)
```

time: 415 us -> 320 us (0.77)
  Pallas kernels: 0 us -> 99 us
  waiting for transfers between devices: 192 us -> 110 us
  local copies, waits for them, and re-layouts: 69.4 us -> 20.2 us
  matrix products: 58.7 us -> 18.4 us
  blocking collectives: 0 us -> 37.8 us
  other arithmetic: 39.7 us -> 8.38 us
  starting transfers between devices: 27.5 us -> 8.04 us
  loops' own time: 12.2 us -> 0 us
    pallas_call x0 -> x1, Pallas kernels: none -> 99 us  [attention(): pl.pallas_call(attention_kernel, out_shape=jax.ShapeDtypeStruct((128, wid...]
    ppermute x10 -> x0, waiting for transfers between devices: 53.1 us -> none  [from_partner(): return lax.ppermute(block, axis, route)]
    dot_general x41 -> x3, matrix products: 58.7 us -> 18.4 us  [the longest x1 10.6 us: experts_part(): jnp.dot(hidden, down_weight[0], preferred_element_type=f32).astype(bf16)]
    all_to_all x0 -> x1, blocking collectives: none -> 37.8 us  [experts_part(): lax.all_to_all(outgoing, 'ep', split_axis=0, concat_axis=0, tiled=True)]
    all_to_all x2 -> x1, waiting for transfers between devices: 26.1 us -> 0.01 us  [experts_part(): lax.all_to_all(results, 'ep', split_axis=0, concat_axis=0, tiled=True)]
    reduce_sum x13 -> x3, other arithmetic: 27.6 us -> 6.92 us  [the longest x1 5.59 us: experts_part(): jnp.sum(picked.astype(f32) * route_weights[:, :, None], axis=1).astype(bf16)]
    reduce_scatter x1, waiting for transfers between devices: 74.6 us -> 56.1 us  [experts_part(): lax.psum_scatter(expert_term, 'tp', scatter_dimension=0, tiled=True)]
    all_gather x2 -> x1, waiting for transfers between devices: 37.8 us -> 54.3 us  [experts_part(): shard_rows = lax.all_gather(arrived, 'tp', axis=0, tiled=True)]
  transfers between devices with their start and end apart: 15 -> 3, of which waited for: 12 -> 2; matrix products, arithmetic and copies ran while one was open for 32% -> 0% of each run, Pallas kernels for 0% -> 31%
where the time goes in v1:
time: 320 us; the launch traced here: 317 us
  waiting for transfers between devices  110 us (34%)
  Pallas kernels  99 us (31%)
  blocking collectives  37.8 us (12%)
  local copies, waits for them, and re-layouts  20.2 us (6%)
  matrix products  18.4 us (6%)
  between operations  14.3 us (4%)
  other arithmetic  8.38 us (3%)
  starting transfers between devices  8.04 us (3%)
    pallas_call x1, Pallas kernels, attention(): pl.pallas_call(attention_kernel, out_shape=jax.ShapeDtypeStruct((128, wid...  99 us
    reduce_scatter x1, waiting for transfers between devices, experts_part(): lax.psum_scatter(expert_term, 'tp', scatter_dimension=0, tiled=True)  56.1 us
    all_gather x1, waiting for transfers between devices, experts_part(): shard_rows = lax.all_gather(arrived, 'tp', axis=0, tiled=True)  54.3 us
    all_to_all x1, blocking collectives, experts_part(): lax.all_to_all(outgoing, 'ep', split_axis=0, concat_axis=0, tiled=True)  37.8 us
    dot_general x1, matrix products, experts_part(): jnp.dot(hidden, down_weight[0], preferred_element_type=f32).astype(bf16)  10.6 us
    all_to_all x1, starting transfers between devices, experts_part(): lax.all_to_all(results, 'ep', split_axis=0, concat_axis=0, tiled=True)  7.96 us
  transfers between devices with their start and end apart: 3, of which 2 were waited for; matrix products, arithmetic and copies ran while one was open for 0% of the time, Pallas kernels for 31%

profile of v1, /device:TPU:1, one launch (start us, length us, event | category | flops | bytes accessed | tf_op | source)
XLA Modules:
  0.0 316.5 jit_solution(4923994449745191171)
XLA Ops:
  7.2 0.9 copy.21
  8.1 0.7 broadcast_multiply_fusion.1
  8.8 0.1 eq.43
  9.0 0.1 eq.39
  9.1 0.6 reduce-window.6
  9.7 0.2 slice_reduce_fusion
  10.1 0.1 reduce_sum.32
  10.4 1.2 fusion.1
  11.6 2.7 convolution_convert_fusion.1
  14.3 2.3 all_to_all.16
  16.6 37.8 %all_to_all.24 = bf16[32,10,2048]{2,1,0:T(8,128)(2,1)} all-to-all(bf16[32,10,2048]{2,1,0:T(8,128)(2,1)S(1)} %all_to_all.16), channel_id=1, replica_groups=mesh['ep'=32,'tp'=4] {'ep'}, dimensions={0} | all-to-all | bytes 2621440 | tf_op jit(solution)/shard_map/all_to_all | solution.py:454
  54.4 3.7 %all_to_all.18 = bf16[320,2048]{1,0:T(8,128)(2,1)} reshape(bf16[32,10,2048]{2,1,0:T(8,128)(2,1)} %all_to_all.24) | data formatting | bytes 2621440 | tf_op jit(solution)/shard_map/all_to_all | solution.py:454
  58.1 54.3 %all-gather.2.cloned.1.call-done = bf16[1280,2048]{1,0:T(8,128)(2,1)} async-done(((bf16[320,2048]{1,0:T(8,128)(2,1)}), bf16[1280,2048]{1,0:T(8,128)(2,1)}) %all-gather.2.cloned.1.call-update) | async-done | bytes 5242896 | tf_op jit(solution)/shard_map/all_gather | solution.py:455
  112.4 5.1 %fusion.7 = f32[1280,256]{1,0:T(8,128)} fusion(bf16[1280,2048]{1,0:T(8,128)(2,1)} %all-gather.2.cloned.1.call-done, bf16[1,2048,256]{2,1,0:T(8,128)(2,1)S(1)} %copy-done.8), kind=kOutput, calls=%fused_computation.13 | convolution fusion | flops 1342177280 | bytes 7602176 | tf_op jit(solution)/shard_map/dot_general | solution.py:456
  117.5 10.6 %convolution_convert_fusion = bf16[1280,2048]{1,0:T(8,128)(2,1)} fusion(bf16[1280,2048]{1,0:T(8,128)(2,1)} %all-gather.2.cloned.1.call-done, f32[1280,256]{1,0:T(8,128)} %fusion.7, bf16[1,256,2048]{2,1,0:T(8,128)(2,1)S(1)} %copy-done, bf16[1,2048,256]{2,1,0:T(8,128)(2,1)S(1)} %copy-done.9), kind=kOutput, calls=%fused_computation.1 | convolution fusion | flops 2688942080 | bytes 13893632 | tf_op jit(solution)/shard_map/dot_general | solution.py:459
  128.1 56.1 %reduce-scatter.2.cloned.1.call-done = bf16[320,2048]{1,0:T(8,128)(2,1)} async-done(((bf16[1280,2048]{1,0:T(8,128)(2,1)}), bf16[320,2048]{1,0:T(8,128)(2,1)}) %reduce-scatter.2.cloned.1.call-update) | async-done | bytes 1310736 | tf_op jit(solution)/shard_map/reduce_scatter | solution.py:460
  184.3 3.3 %all_to_all.19 = bf16[32,10,2048]{2,1,0:T(8,128)(2,1)} reshape(bf16[320,2048]{1,0:T(8,128)(2,1)} %reduce-scatter.2.cloned.1.call-done) | data formatting | bytes 2621440 | tf_op jit(solution)/shard_map/all_to_all | solution.py:461
  187.7 8.0 %all-to-all-start.1 = ((bf16[32,10,2048]{2,1,0:T(8,128)(2,1)}), bf16[32,10,2048]{2,1,0:T(8,128)(2,1)}, u32[]{:S(2)}, u32[]{:S(2)}) async-start(bf16[32,10,2048]{2,1,0:T(8,128)(2,1)} %all_to_all.19), calls=%async_computation.2 | async-start | bytes 4194304 | tf_op jit(solution)/shard_map/all_to_all | solution.py:461
  196.0 99.0 %attention.1 = bf16[128,2048]{1,0:T(8,128)(2,1)S(1)} custom-call(bf16[512,256]{1,0:T(8,128)(2,1)S(1)} %copy-done.2, bf16[512,256]{1,0:T(8,128)(2,1)S(1)} %copy-done.3, bf16[512,256]{1,0:T(8,128)(2,1)S(1)} %copy-done.4, f32[2]{0:T(128)S(1)} %copy-done.5, f32[1,128]{1,0:T(1,128)S(1)} %bitcast.33, bf16[2,128,2048]{2,1,0:T(8,128)(2,1)S(1)} %bitcast.32), custom_call_target="tpu_custom_call" | custom-call | tf_op jit(solution)/shard_map/attention/pallas_call | solution.py:392
  295.0 2.5 all_to_all.21
  297.5 2.3 gather_fusion
  299.9 3.4 %reshape.94 = f32[128,2,2048]{2,1,0:T(2,128)} reshape(bf16[256,2048]{1,0:T(8,128)(2,1)} %gather_fusion) | data formatting | bytes 3145728 | tf_op jit(solution)/shard_map/convert_element_type | solution.py:463
  303.3 5.6 %multiply_reduce_fusion = bf16[128,2048]{1,0:T(8,128)(2,1)} fusion(f32[128,2,2048]{2,1,0:T(2,128)} %reshape.94, f32[128,2]{1,0:T(8,128)S(1)} %copy.24), kind=kLoop, calls=%fused_computation.5 | loop fusion | flops 786432 | bytes 2622464 | tf_op jit(solution)/shard_map/reduce_sum | solution.py:463
  308.9 0.8 copy.28
  (38 shorter events, 0.8 us)
Async XLA Ops:
  7.2 110.3 %copy-start = (bf16[1,256,2048]{2,1,0:T(8,128)(2,1)S(1)}, bf16[1,256,2048]{2,1,0:T(8,128)(2,1)}, u32[]{:S(2)}) copy-start(bf16[1,256,2048]{2,1,0:T(8,128)(2,1)} %param.27) | copy-start | bytes 3145732
  7.2 105.2 %all-gather.2.cloned.1.call-start = ((), (), s32[]{:S(2)}) async-start(), calls=%async_computation.3 | async-start | bytes 6553600 | tf_op jit(solution)/shard_map/all_gather | solution.py:455
  54.4 58.0 %copy-start.8 = (bf16[1,2048,256]{2,1,0:T(8,128)(2,1)S(1)}, bf16[1,2048,256]{2,1,0:T(8,128)(2,1)}, u32[]{:S(2)}) copy-start(bf16[1,2048,256]{2,1,0:T(8,128)(2,1)} %param.25) | copy-start | bytes 3145732
  58.1 59.4 %copy-start.9 = (bf16[1,2048,256]{2,1,0:T(8,128)(2,1)S(1)}, bf16[1,2048,256]{2,1,0:T(8,128)(2,1)}, u32[]{:S(2)}) copy-start(bf16[1,2048,256]{2,1,0:T(8,128)(2,1)} %param.26) | copy-start | bytes 3145732
  58.1 126.2 %reduce-scatter.2.cloned.1.call-start = ((), (), s32[]{:S(2)}) async-start(), calls=%async_computation.4 | async-start | bytes 6553600 | tf_op jit(solution)/shard_map/reduce_scatter | solution.py:460
  187.6 8.2 %copy-start.7 = (f32[128,2]{0,1:T(2,128)S(1)}, f32[128,2]{0,1:T(2,128)}, u32[]{:S(2)}) copy-start(f32[128,2]{0,1:T(2,128)} %param.24) | copy-start | bytes 3076
  187.6 8.3 %copy-start.1 = (bf16[256,2048]{1,0:T(8,128)(2,1)S(1)}, bf16[256,2048]{1,0:T(8,128)(2,1)}, u32[]{:S(2)}) copy-start(bf16[256,2048]{1,0:T(8,128)(2,1)} %param.19) | copy-start | bytes 3145732
  187.6 8.3 %copy-start.2 = (bf16[512,256]{1,0:T(8,128)(2,1)S(1)}, bf16[512,256]{1,0:T(8,128)(2,1)}, u32[]{:S(2)}) copy-start(bf16[512,256]{1,0:T(8,128)(2,1)} %q_ref.1) | copy-start | bytes 786436
  187.6 8.3 %copy-start.3 = (bf16[512,256]{1,0:T(8,128)(2,1)S(1)}, bf16[512,256]{1,0:T(8,128)(2,1)}, u32[]{:S(2)}) copy-start(bf16[512,256]{1,0:T(8,128)(2,1)} %k_ref.1) | copy-start | bytes 786436
  187.6 8.3 %copy-start.4 = (bf16[512,256]{1,0:T(8,128)(2,1)S(1)}, bf16[512,256]{1,0:T(8,128)(2,1)}, u32[]{:S(2)}) copy-start(bf16[512,256]{1,0:T(8,128)(2,1)} %v_ref.1) | copy-start | bytes 786436
  187.6 8.3 %copy-start.5 = (f32[2]{0:T(128)S(1)}, f32[2]{0:T(128)}, u32[]{:S(2)}) copy-start(f32[2]{0:T(128)} %lam_ref.1) | copy-start | bytes 28
  187.7 8.3 %copy-start.6 = (f32[128]{0:T(128)S(1)}, f32[128]{0:T(128)}, u32[]{:S(2)}) copy-start(f32[128]{0:T(128)} %param.18) | copy-start | bytes 1540
  187.7 107.3 %all-to-all-start.1 = ((bf16[32,10,2048]{2,1,0:T(8,128)(2,1)}), bf16[32,10,2048]{2,1,0:T(8,128)(2,1)}, u32[]{:S(2)}, u32[]{:S(2)}) async-start(bf16[32,10,2048]{2,1,0:T(8,128)(2,1)} %all_to_all.19), calls=%async_computation.2 | async-start | bytes 4194304 | tf_op jit(solution)/shard_map/all_to_all | solution.py:461
Sparse Core Ops, SparseCore 0:
  58.2 54.1 all-gather.1
  128.3 55.9 reduce-scatter.1

commit v2 on v1

--- a/solution.py
+++ b/solution.py
@@ -11,6 +11,10 @@
 GROUPS = 4
 SIDE = 4
 CHIPS = 16
+SLOTS = 320
+ROWS = 80
+BATCH = ROWS * 16
+CHUNK = 160
 MESH = pl.DeviceIdType.MESH
 
 eps = 1e-06
@@ -23,14 +27,22 @@
     return lax.rem(v + SIDE, SIDE)
 
 
-def attention_kernel(
+def layer_kernel(
     q_ref,
     k_ref,
     v_ref,
     lam_ref,
     gain_ref,
     ow_ref,
+    tok_ref,
+    norm_ref,
+    place_ref,
+    mix_ref,
+    gate_ref,
+    up_ref,
+    down_ref,
     out_ref,
+    comb_ref,
     kv,
     give,
     qb,
@@ -50,6 +62,31 @@
     ow_recv,
     head_send,
     head_recv,
+    gate_w,
+    up_w,
+    down_w,
+    wide,
+    normed_tok,
+    rows_in,
+    slots,
+    routed,
+    partial,
+    far_sum,
+    near_sum,
+    results,
+    returned,
+    weights_here,
+    self_here,
+    out_send,
+    out_recv,
+    gather_send,
+    gather_recv,
+    far_send,
+    far_recv,
+    near_send,
+    near_recv,
+    back_send,
+    back_recv,
 ):
     ep = lax.axis_index("ep")
     x = lax.axis_index("tp")
@@ -108,7 +145,168 @@
     half_of = kv.at[chip, pl.ds(2 * core, 2)]
     give_kv = remote(give, half_of, pre_send.at[0], pre_recv.at[0], partner)
     give_kv.start()
+    weight_copies = [
+        pltpu.make_async_copy(a, b, weights_here.at[n])
+        for n, (a, b) in enumerate(((gate_ref, gate_w), (up_ref, up_w), (down_ref, down_w)))
+    ]
+    for c in weight_copies:
+        c.start()
+
+    tok = tok_ref[...].astype(f32)
+    mean_tok = jnp.mean(tok * tok, axis=1, keepdims=True)
+    normed_tok[...] = (tok * lax.rsqrt(mean_tok + eps) * norm_ref[...]).astype(bf16)
+    for cb in range(16):
+        wide[pl.ds(cb, SLOTS, stride=16), :] = jnp.dot(
+            place_ref[...], normed_tok[:, cb * 128 : (cb + 1) * 128], preferred_element_type=f32
+        )
+
+    def to_slots(n, carry):
+        at = pl.ds(pl.multiple_of(n * BATCH, BATCH), BATCH)
+        slots[at, :] = wide[at, :].astype(bf16)
+        return carry
+
+    lax.fori_loop(0, 4, to_slots, 0)
+
+    def chunk(e):
+        return pl.ds(pl.multiple_of(e * CHUNK, CHUNK), CHUNK)
+
+    def batch_rows(k):
+        return pl.ds(pl.multiple_of(wrap(at_z - k) * BATCH, BATCH), BATCH)
+
+    def plane_member(k, n):
+        return chip_at(k, n // 2) * 2 + lax.rem(core + n % 2, 2)
+
+    def dispatch(k, n):
+        e = plane_member(k, n)
+        return remote(
+            slots.at[chunk(e)], routed.at[x, chunk(ep)], out_send.at[k, n], out_recv.at[k, n], (e, x)
+        )
+
+    pairs = [(k, n) for k in range(4) for n in range(8)]
+    own_slots = pltpu.make_async_copy(slots.at[chunk(ep)], routed.at[x, chunk(ep)], self_here.at[0])
+    own_slots.start()
+    for k, n in pairs[1:]:
+        dispatch(k, n).start()
     lay_out(core, put_own)
+
+    def x_copy(xs, k, slot):
+        at = routed.at[xs, batch_rows(k)]
+        return remote(at, at, gather_send.at[k, slot], gather_recv.at[k, slot], (ep, right if slot in (0, 2) else left))
+
+    def gather_right(k):
+        return x_copy(x, k, 0)
+
+    def gather_left(k):
+        return x_copy(x, k, 1)
+
+    def gather_relay(k):
+        at = routed.at[left if k < 2 else right, batch_rows(k)]
+        return remote(at, at, gather_send.at[k, 2], gather_recv.at[k, 2], (ep, right if k < 2 else left))
+
+    def expert_term(xs, k):
+        rows = pl.ds(0, BATCH)
+        wide[rows, :] = routed[xs, batch_rows(k), :].astype(f32)
+        for cb in range(16):
+            rows_in[:, cb * 128 : (cb + 1) * 128] = wide[pl.ds(cb, ROWS, stride=16), :].astype(bf16)
+        gate = jnp.dot(rows_in[...], gate_w[...], preferred_element_type=f32)
+        up = jnp.dot(rows_in[...], up_w[...], preferred_element_type=f32)
+        hidden = (jax.nn.silu(gate) * up).astype(bf16)
+        for cb in range(8):
+            part = jnp.dot(hidden, down_w[:, cb * 256 : (cb + 1) * 256], preferred_element_type=f32)
+            wide[pl.ds(2 * cb, ROWS, stride=16), :] = part[:, :128]
+            wide[pl.ds(2 * cb + 1, ROWS, stride=16), :] = part[:, 128:]
+
+    def send_far(k):
+        return remote(
+            partial.at[2, k], far_sum.at[k], far_send.at[k], far_recv.at[k], (ep, left if k < 2 else right)
+        )
+
+    def send_left(k):
+        return remote(partial.at[0, k], near_sum.at[1, k], near_send.at[0, k], near_recv.at[1, k], (ep, left))
+
+    def send_right(k):
+        return remote(partial.at[1, k], near_sum.at[0, k], near_send.at[1, k], near_recv.at[0, k], (ep, right))
+
+    def send_back(k, n):
+        e = plane_member(-k, n)
+        place = 2 * wrap(at_y + n // 2) + lax.rem(core + n % 2, 2)
+        return remote(
+            results.at[k, chunk(place)], returned.at[chunk(ep)], back_send.at[k, n], back_recv.at[k, n], (e, x)
+        )
+
+    def step_a(k):
+        for n in range(8):
+            if (k, n) == (0, 0):
+                own_slots.wait()
+            else:
+                dispatch(k, n).wait_recv()
+        gather_right(k).start()
+        gather_left(k).start()
+
+    def step_b(k):
+        gather_right(k).wait_recv()
+        gather_left(k).wait_recv()
+        gather_relay(k).start()
+        if k < 2:
+            expert_term(right, k)
+            partial[1, k] = wide[0:BATCH, :].astype(bf16)
+            send_right(k).start()
+        else:
+            expert_term(left, k)
+            partial[0, k] = wide[0:BATCH, :].astype(bf16)
+            send_left(k).start()
+
+    def step_c(k):
+        gather_relay(k).wait_recv()
+        expert_term(far, k)
+        partial[2, k] = wide[0:BATCH, :].astype(bf16)
+        send_far(k).start()
+
+    def step_d(k):
+        side = 0 if k < 2 else 1
+        expert_term(left if k < 2 else right, k)
+        send_far(k).wait_recv()
+        partial[side, k] = (wide[0:BATCH, :] + far_sum[k].astype(f32)).astype(bf16)
+        (send_left if k < 2 else send_right)(k).start()
+
+    def step_e(k):
+        expert_term(x, k)
+        send_left(k).wait_recv()
+        send_right(k).wait_recv()
+        results[k] = (
+            wide[0:BATCH, :] + (near_sum[0, k].astype(f32) + near_sum[1, k].astype(f32))
+        ).astype(bf16)
+        for n in range(8):
+            if (k, n) == (0, 0):
+                pltpu.make_async_copy(
+                    results.at[0, chunk(2 * at_y + core)], returned.at[chunk(ep)], self_here.at[1]
+                ).start()
+            else:
+                send_back(k, n).start()
+
+    def step_f():
+        for k, n in pairs:
+            if (k, n) == (0, 0):
+                pltpu.make_async_copy(
+                    results.at[0, chunk(2 * at_y + core)], returned.at[chunk(ep)], self_here.at[1]
+                ).wait()
+            else:
+                send_back(k, n).wait_recv()
+
+        def widen(n, carry):
+            at = pl.ds(pl.multiple_of(n * BATCH, BATCH), BATCH)
+            wide[at, :] = returned[at, :].astype(f32)
+            return carry
+
+        lax.fori_loop(0, 4, widen, 0)
+        high = mix_ref[...].astype(bf16)
+        low = (mix_ref[...] - high.astype(f32)).astype(bf16)
+        for cb in range(16):
+            got = wide[pl.ds(cb, SLOTS, stride=16), :].astype(bf16)
+            total = jnp.dot(high, got, preferred_element_type=f32) + jnp.dot(
+                low, got, preferred_element_type=f32
+            )
+            comb_ref[:, cb * 128 : (cb + 1) * 128] = total.astype(bf16)
 
     def step_to(axis, sign):
         return chip_at(sign, 0) if axis == 0 else chip_at(0, sign)
@@ -282,8 +480,15 @@
                 phase[half][n][0].start()
                 phase[half][n][1].start()
 
+    for c in weight_copies:
+        c.wait()
+    own_late = jnp.where(chip < mirror, chip, CHIPS)
     unit(0, chip, 0, True)
-    batch([(jnp.where(chip < mirror, chip, CHIPS), 0), (jnp.where(chip < mirror, chip, CHIPS), 1)])
+    step_a(0)
+    step_a(1)
+    batch([(own_late, 0), (own_late, 1)])
+    step_a(2)
+    step_a(3)
     direct((0,))
     begin((2, 3))
     batch(arrivals((0,), (-1, 1)))
@@ -296,19 +501,32 @@
     ow_left.wait_recv()
     on_left.start()
     across_copies[1].start()
+    step_b(0)
     batch(arrivals((0,), (2,)) + arrivals((1,), (-1, 1)))
     direct((2, 3))
-    batch(arrivals((2,), (-1, 1)) + arrivals((3,), (-1, 1)))
+    step_b(1)
+    batch(arrivals((2,), (-1, 1)))
+    step_b(2)
+    batch(arrivals((3,), (-1, 1)))
+    step_b(3)
     relayed((1,))
     direct((4,))
     on_right.wait_recv()
     on_left.wait_recv()
     across_copies[2].start()
+    step_c(0)
     batch(arrivals((1,), (2,)) + arrivals((4,), (-1, 1)))
     relayed((2, 3, 4))
+    step_c(1)
     batch(arrivals((2,), (2,)) + arrivals((3,), (2,)) + arrivals((4,), (2,)))
+    step_c(2)
+    step_c(3)
+    step_d(0)
     unit(1, mirror, 0, False)
+    step_d(1)
     unit(1, mirror, 1, True)
+    step_d(2)
+    step_d(3)
 
     lam = lam_ref[core]
 
@@ -342,6 +560,8 @@
             else:
                 to_owner(1, n, 2 * mirror + 1).start()
 
+    for k in range(4):
+        step_e(k)
     keep_ow.wait()
     for c in across_copies:
         c.wait_recv()
@@ -361,6 +581,7 @@
         return carry
 
     lax.fori_loop(0, 4, project, 0)
+    step_f()
 
     give_kv.wait_send()
 
@@ -375,6 +596,12 @@
 
     for c in sent + [ow_right, ow_left, on_right, on_left] + across_copies:
         c.wait_send()
+    for k, n in pairs[1:]:
+        dispatch(k, n).wait_send()
+        send_back(k, n).wait_send()
+    for k in range(4):
+        for c in (gather_right(k), gather_left(k), gather_relay(k), send_far(k), send_left(k), send_right(k)):
+            c.wait_send()
     for n in range(4):
 
         @pl.when(jnp.logical_not(home(n)))
@@ -384,16 +611,19 @@
         to_owner(1, n, 2 * mirror + 1).wait_send()
 
 
-def attention(query_rows, key_rows, value_rows, lambdas, out_gain, out_weight):
+def layer(query_rows, key_rows, value_rows, lambdas, out_gain, out_weight, tokens, norm_gain, place, mix, weights):
     any_space = pl.BlockSpec(memory_space=pl.ANY)
     vmem = pl.BlockSpec(memory_space=pltpu.VMEM)
     width = out_weight.shape[1]
     dma = pltpu.SemaphoreType.DMA
+    shape = jax.ShapeDtypeStruct((128, width), bf16)
     return pl.pallas_call(
-        attention_kernel,
-        out_shape=jax.ShapeDtypeStruct((128, width), bf16),
-        in_specs=[any_space, vmem, vmem, pl.BlockSpec(memory_space=pltpu.SMEM), vmem, any_space],
-        out_specs=vmem,
+        layer_kernel,
+        out_shape=(shape, shape),
+        in_specs=[any_space, vmem, vmem, pl.BlockSpec(memory_space=pltpu.SMEM), vmem, any_space]
+        + [vmem] * 4
+        + [any_space] * 3,
+        out_specs=(vmem, vmem),
         scratch_shapes=[
             pltpu.VMEM((CHIPS, 4, 512, 128), bf16),
             pltpu.VMEM((2, 512, 128), bf16),
@@ -414,9 +644,34 @@
             dma((7,)),
             dma((2, 4)),
             dma((8,)),
+            pltpu.VMEM((width, 256), bf16),
+            pltpu.VMEM((width, 256), bf16),
+            pltpu.VMEM((256, width), bf16),
+            pltpu.VMEM((4 * BATCH, 128), f32),
+            pltpu.VMEM((128, width), bf16),
+            pltpu.VMEM((ROWS, width), bf16),
+            pltpu.VMEM((4 * BATCH, 128), bf16),
+            pltpu.VMEM((4, 4 * BATCH, 128), bf16),
+            pltpu.VMEM((3, 4, BATCH, 128), bf16),
+            pltpu.VMEM((4, BATCH, 128), bf16),
+            pltpu.VMEM((2, 4, BATCH, 128), bf16),
+            pltpu.VMEM((4, BATCH, 128), bf16),
+            pltpu.VMEM((4 * BATCH, 128), bf16),
+            dma((3,)),
+            dma((2,)),
+            dma((4, 8)),
+            dma((4, 8)),
+            dma((4, 3)),
+            dma((4, 3)),
+            dma((4,)),
+            dma((4,)),
+            dma((2, 4)),
+            dma((2, 4)),
+            dma((4, 8)),
+            dma((4, 8)),
         ],
-        compiler_params=pltpu.CompilerParams(has_side_effects=True, vmem_limit_bytes=40 * 2**20),
-        name="attention",
+        compiler_params=pltpu.CompilerParams(has_side_effects=True, vmem_limit_bytes=60 * 2**20),
+        name="layer",
     )(
         query_rows,
         key_rows,
@@ -424,43 +679,29 @@
         lambdas,
         out_gain.reshape(1, -1),
         out_weight.reshape(2, 128, width),
+        tokens,
+        norm_gain.reshape(1, -1),
+        place,
+        mix,
+        *weights,
     )
 
 
-def experts_part(
-    tokens, norm_gain, group_ids, inner_ids, route_weights, gate_weight, up_weight, down_weight
-):
-    tok_dev = tokens.shape[0]
-    model_width = tokens.shape[1]
-    topk_count = inner_ids.shape[1]
+def routing(group_ids, inner_ids, route_weights):
+    tok_dev, topk_count = inner_ids.shape
     experts = lax.axis_size("ep")
     group_size = experts // GROUPS
     capacity = 5 * tok_dev * topk_count // (4 * experts)
-    tok_wide = tokens.astype(f32)
-    normed = (
-        tok_wide * lax.rsqrt(jnp.mean(tok_wide * tok_wide, axis=1, keepdims=True) + eps) * norm_gain
-    ).astype(bf16)
     target = (group_ids[:, None] * group_size + inner_ids).reshape(-1)
     labels = jnp.arange(experts, dtype=jnp.int32)
     onehot = (target[:, None] == labels[None, :]).astype(jnp.int32)
     slot_rank = jnp.sum((jnp.cumsum(onehot, axis=0) - 1) * onehot, axis=1)
-    slot_of = target * capacity + slot_rank
+    slot_of = (target * capacity + slot_rank).reshape(tok_dev, topk_count)
     slot_ids = jnp.arange(experts * capacity, dtype=jnp.int32)
-    placing = jnp.any(
-        (slot_of[:, None] == slot_ids[None, :]).reshape(tok_dev, topk_count, experts * capacity),
-        axis=1,
-    ).astype(bf16)
-    outgoing = jnp.einsum("ts,td->sd", placing, normed, preferred_element_type=f32).astype(bf16)
-    arrived = lax.all_to_all(outgoing, "ep", split_axis=0, concat_axis=0, tiled=True)
-    shard_rows = lax.all_gather(arrived, "tp", axis=0, tiled=True)
-    gate_pre = jnp.dot(shard_rows, gate_weight[0], preferred_element_type=f32)
-    up_pre = jnp.dot(shard_rows, up_weight[0], preferred_element_type=f32)
-    hidden = (jax.nn.silu(gate_pre) * up_pre).astype(bf16)
-    expert_term = jnp.dot(hidden, down_weight[0], preferred_element_type=f32).astype(bf16)
-    results = lax.psum_scatter(expert_term, "tp", scatter_dimension=0, tiled=True)
-    returned = lax.all_to_all(results, "ep", split_axis=0, concat_axis=0, tiled=True)
-    picked = returned[slot_of].reshape(tok_dev, topk_count, model_width)
-    return jnp.sum(picked.astype(f32) * route_weights[:, :, None], axis=1).astype(bf16)
+    place = jnp.any(slot_ids[:, None, None] == slot_of[None], axis=2).astype(bf16)
+    chosen = slot_of[:, :, None] == slot_ids[None, None, :]
+    mix = jnp.sum(jnp.where(chosen, route_weights[:, :, None], 0.0), axis=1)
+    return place, mix
 
 
 def body(
@@ -479,11 +720,20 @@
     up_weight,
     down_weight,
 ):
-    attended = attention(query_rows, key_rows, value_rows, lambdas, out_gain, out_weight)
-    combined = experts_part(
-        tokens, norm_gain, group_ids, inner_ids, route_weights, gate_weight, up_weight, down_weight
+    place, mix = routing(group_ids, inner_ids, route_weights)
+    return layer(
+        query_rows,
+        key_rows,
+        value_rows,
+        lambdas,
+        out_gain,
+        out_weight,
+        tokens,
+        norm_gain,
+        place,
+        mix,
+        (gate_weight[0], up_weight[0], down_weight[0]),
     )
-    return (attended, combined)
 
 
 def solution(mesh):

time: 320 us -> 161 us (0.50); the launches traced: 317 us -> 161 us
  waiting for transfers between devices: 110 us -> 0 us
  Pallas kernels: 99 us -> 153 us
  blocking collectives: 37.8 us -> 0 us
  matrix products: 18.4 us -> 0 us
  local copies, waits for them, and re-layouts: 20.2 us -> 5.67 us
  between operations: 14.3 us -> 0.72 us
  starting transfers between devices: 8.04 us -> 0 us
  other arithmetic: 8.38 us -> 1.65 us
    reduce_scatter x1 -> x0, waiting for transfers between devices: 56.1 us -> none  [experts_part(): lax.psum_scatter(expert_term, 'tp', scatter_dimension=0, tiled=True)]
    all_gather x1 -> x0, waiting for transfers between devices: 54.3 us -> none  [experts_part(): shard_rows = lax.all_gather(arrived, 'tp', axis=0, tiled=True)]
    pallas_call x1, Pallas kernels: 99 us -> 153 us  [layer(): pl.pallas_call(layer_kernel, out_shape=(shape, shape), in_specs=[any_spac...]
    all_to_all x1 -> x0, blocking collectives: 37.8 us -> none  [experts_part(): lax.all_to_all(outgoing, 'ep', split_axis=0, concat_axis=0, tiled=True)]
    dot_general x3 -> x0, matrix products: 18.4 us -> none  [the longest x1 10.6 us: experts_part(): jnp.dot(hidden, down_weight[0], preferred_element_type=f32).astype(bf16)]
    all_to_all x4 -> x0, local copies, waits for them, and re-layouts: 11.8 us -> none  [the longest x2 5.97 us: experts_part(): lax.all_to_all(outgoing, 'ep', split_axis=0, concat_axis=0, tiled=True)]
    all_to_all x1 -> x0, starting transfers between devices: 7.96 us -> none  [experts_part(): lax.all_to_all(results, 'ep', split_axis=0, concat_axis=0, tiled=True)]
    reduce_sum x3 -> x2, other arithmetic: 6.92 us -> 0.13 us  [the longest x1 0.1 us: routing(): slot_rank = jnp.sum((jnp.cumsum(onehot, axis=0) - 1) * onehot, axis=1)]
  transfers between devices with their start and end apart: 3 -> 0, of which waited for: 2 -> 0; matrix products, arithmetic and copies ran while one was open for 0% -> 0% of each run, Pallas kernels for 31% -> 0%
where the time goes in v2:
time: 161 us
  Pallas kernels  153 us (95%)
  local copies, waits for them, and re-layouts  5.67 us (4%)
  other arithmetic  1.65 us (1%)
    pallas_call x1, Pallas kernels, layer(): pl.pallas_call(layer_kernel, out_shape=(shape, shape), in_specs=[any_spac...  153 us
    unnamed x11, local copies, waits for them, and re-layouts  4.19 us

profile of v2, /device:TPU:1, one launch (start us, length us, event | category | flops | bytes accessed | tf_op | source)
XLA Modules:
  0.0 161.1 jit_solution(17231117647336844327)
XLA Ops:
  0.6 0.0 copy-start.3
  0.6 0.6 copy-done.3
  1.3 0.0 copy-start.1
  1.3 0.7 copy-done.1
  2.0 0.1 copy.22
  2.1 0.1 broadcast_add_fusion
  2.2 0.1 eq.52
  2.3 0.1 eq.56
  2.5 0.6 reduce-window.6
  3.1 0.2 slice_reduce_fusion
  3.3 0.1 fusion.2
  3.4 0.1 reduce_sum.21
  3.5 0.1 multiply_add_fusion
  3.6 0.1 copy.24
  3.7 0.1 fusion
  3.8 0.0 copy-start.2
  3.8 0.7 convert_element_type.9.place_ref
  4.4 0.0 copy-done.2
  4.5 0.8 copy.26.mix_ref
  5.3 153.0 %layer.1 = (bf16[128,2048]{1,0:T(8,128)(2,1)}, bf16[128,2048]{1,0:T(8,128)(2,1)}) custom-call(bf16[512,256]{1,0:T(8,128)(2,1)} %q_ref.1, bf16[512,256]{1,0:T(8,128)(2,1)} %k_ref.1, bf16[512,256]{1,0:T(8,128)(2,1)} %v_ref.1, f32[2]{0:T(128)} %lam_ref.1, f32[1,128]{1,0:T(1,128)} %bitcast.26, bf16[2,128,2048]{2,1,0:T(8,128)(2,1)} %bitcast.21, ...), custom_call_target="tpu_custom_call" | custom-call | tf_op jit(solution)/shard_map/layer/pallas_call | solution.py:620
  158.3 0.0 copy-start
  158.3 1.9 %copy.31 = bf16[128,2048]{1,0:T(8,128)(2,1)} copy(bf16[128,2048]{1,0:T(8,128)(2,1)} %get-tuple-element.4) | data formatting | bytes 1048576
  160.3 0.0 copy-done
  160.3 0.8 copy.32
  (5 shorter events, 0.1 us)
Async XLA Ops:
  0.6 0.7 copy-start.3
  1.3 0.7 copy-start.1
  3.8 0.7 copy-start.2
  158.3 2.0 %copy-start = (bf16[128,2048]{1,0:T(8,128)(2,1)S(1)}, bf16[128,2048]{1,0:T(8,128)(2,1)}, u32[]{:S(2)}) copy-start(bf16[128,2048]{1,0:T(8,128)(2,1)} %get-tuple-element.5) | copy-start | bytes 1572868

commit v3 on v2

--- a/solution.py
+++ b/solution.py
@@ -51,6 +51,7 @@
     top,
     tot,
     ow,
+    ow_mate,
     heads,
     outgoing,
     pre_send,
@@ -111,40 +112,20 @@
 
     partner = (2 * chip + mate, x)
 
-    keep_q = pltpu.make_async_copy(q_ref.at[:, cols(0)], qb.at[0], here.at[0])
-    give_q = remote(q_ref.at[:, cols(1)], qb.at[0], pre_send.at[1], pre_recv.at[1], partner)
-    far_q = [
-        remote(q_ref.at[:, cols(h)], qb.at[1], pre_send.at[1 + h], pre_recv.at[2], (2 * mirror + h, x))
-        for h in range(2)
-    ]
-
-    @pl.when(core == 0)
-    def _():
-        keep_q.start()
-        give_q.start()
-
-    @pl.when(core == 1)
-    def _():
-        far_q[0].start()
-        far_q[1].start()
-
-    def lay_out(head, put):
-        for p in range(2):
-            put(p, pl.ds(0, 256), k_ref[pl.ds(p * 256, 256), cols(head)])
-            for n in range(2):
-                block = v_ref[pl.ds(p * 256 + n * 128, 128), cols(head)].astype(f32)
-                put(p, pl.ds(256 + n * 128, 128), block.T.astype(bf16))
-
-    def put_give(p, rows, value):
-        give[p, rows, :] = value
-
-    def put_own(p, rows, value):
-        kv[chip, 2 * core + p, rows, :] = value
-
-    lay_out(mate, put_give)
-    half_of = kv.at[chip, pl.ds(2 * core, 2)]
-    give_kv = remote(give, half_of, pre_send.at[0], pre_recv.at[0], partner)
-    give_kv.start()
+    barrier = pltpu.get_barrier_semaphore()
+
+    def greet(e, at_x):
+        pl.semaphore_signal(barrier, inc=1, device_id=(e, at_x), device_id_type=MESH)
+
+    def greet_all(n, carry):
+        greet(lax.rem(ep + n, 2 * CHIPS), x)
+        return carry
+
+    lax.fori_loop(1, 2 * CHIPS, greet_all, 0)
+    for d in range(1, SIDE):
+        for e in (ep, 2 * chip + mate, 2 * mirror, 2 * mirror + 1):
+            greet(e, wrap(x + d))
+
     weight_copies = [
         pltpu.make_async_copy(a, b, weights_here.at[n])
         for n, (a, b) in enumerate(((gate_ref, gate_w), (up_ref, up_w), (down_ref, down_w)))
@@ -185,8 +166,50 @@
     pairs = [(k, n) for k in range(4) for n in range(8)]
     own_slots = pltpu.make_async_copy(slots.at[chunk(ep)], routed.at[x, chunk(ep)], self_here.at[0])
     own_slots.start()
-    for k, n in pairs[1:]:
-        dispatch(k, n).start()
+    pl.semaphore_wait(barrier, 2 * CHIPS - 1 + 4 * (SIDE - 1))
+
+    def dispatch_plane(k):
+        for n in range(8):
+            if (k, n) != (0, 0):
+                dispatch(k, n).start()
+
+    dispatch_plane(0)
+
+    keep_q = pltpu.make_async_copy(q_ref.at[:, cols(0)], qb.at[0], here.at[0])
+    give_q = remote(q_ref.at[:, cols(1)], qb.at[0], pre_send.at[1], pre_recv.at[1], partner)
+    far_q = [
+        remote(q_ref.at[:, cols(h)], qb.at[1], pre_send.at[1 + h], pre_recv.at[2], (2 * mirror + h, x))
+        for h in range(2)
+    ]
+
+    @pl.when(core == 0)
+    def _():
+        keep_q.start()
+        give_q.start()
+
+    @pl.when(core == 1)
+    def _():
+        far_q[0].start()
+        far_q[1].start()
+
+    def lay_out(head, put):
+        for p in range(2):
+            put(p, pl.ds(0, 256), k_ref[pl.ds(p * 256, 256), cols(head)])
+            for n in range(2):
+                block = v_ref[pl.ds(p * 256 + n * 128, 128), cols(head)].astype(f32)
+                put(p, pl.ds(256 + n * 128, 128), block.T.astype(bf16))
+
+    def put_give(p, rows, value):
+        give[p, rows, :] = value
+
+    def put_own(p, rows, value):
+        kv[chip, 2 * core + p, rows, :] = value
+
+    lay_out(mate, put_give)
+    half_of = kv.at[chip, pl.ds(2 * core, 2), pl.ds(0, 512)]
+    give_kv = remote(give, half_of, pre_send.at[0], pre_recv.at[0], partner)
+    give_kv.start()
+    dispatch_plane(1)
     lay_out(core, put_own)
 
     def x_copy(xs, k, slot):
@@ -247,6 +270,8 @@
         gather_right(k).wait_recv()
         gather_left(k).wait_recv()
         gather_relay(k).start()
+
+    def step_near(k):
         if k < 2:
             expert_term(right, k)
             partial[1, k] = wide[0:BATCH, :].astype(bf16)
@@ -338,42 +363,25 @@
             phase[half][1 + n] = spread(half, 1 + n, moved((0, 0), one, by), two)
     sent = [c for half in range(2) for group in phase[half] for c in group]
 
-    give_kv.wait_recv()
-    for n in range(2):
-        for half in range(2):
-            phase[half][n][0].start()
-            phase[half][n][1].start()
-
-    keep_ow = pltpu.make_async_copy(ow_ref, ow.at[pl.ds(2 * x, 2)], here.at[1])
+    keep_ow = pltpu.make_async_copy(ow_ref, ow, here.at[1])
     keep_ow.start()
 
-    def ow_rows(at_x, c):
-        return ow.at[2 * at_x + c]
-
-    ow_right = remote(ow_ref.at[core], ow_rows(x, core), ow_send.at[0], ow_recv.at[0], (ep, right))
-    ow_left = remote(ow_ref.at[core], ow_rows(x, core), ow_send.at[1], ow_recv.at[1], (ep, left))
-    ow_right.start()
-    ow_left.start()
-    top_half, low_half = pl.ds(0, 64), pl.ds(64, 64)
-    on_right = remote(
-        ow_rows(left, core).at[top_half],
-        ow_rows(left, core).at[top_half],
-        ow_send.at[2],
-        ow_recv.at[2],
-        (ep, right),
+    def ow_copy(d):
+        return remote(
+            ow_ref.at[core, :, cols(chip)],
+            kv.at[chip, 3 - d, pl.ds(512, 128)],
+            ow_send.at[d - 1],
+            ow_recv.at[3 - d],
+            (ep, wrap(x + d)),
+        )
+
+    ow_copies = [ow_copy(d) for d in (1, 2, 3)]
+    for c in ow_copies:
+        c.start()
+    kv[chip, 3, pl.ds(512, 128), :] = jnp.zeros((128, 128), bf16)
+    across = remote(
+        kv.at[:, pl.ds(0, 3), pl.ds(512, 128)], ow_mate, ow_send.at[3], ow_recv.at[3], partner
     )
-    on_left = remote(
-        ow_rows(right, core).at[low_half],
-        ow_rows(right, core).at[low_half],
-        ow_send.at[3],
-        ow_recv.at[3],
-        (ep, left),
-    )
-
-    def across(n, at_x):
-        return remote(ow_rows(at_x, core), ow_rows(at_x, core), ow_send.at[4 + n], ow_recv.at[4 + n], partner)
-
-    across_copies = [across(0, left), across(1, right), across(2, far)]
 
     @pl.when(core == 0)
     def _():
@@ -483,50 +491,55 @@
     for c in weight_copies:
         c.wait()
     own_late = jnp.where(chip < mirror, chip, CHIPS)
+    step_a(0)
+    dispatch_plane(2)
+    give_kv.wait_recv()
     unit(0, chip, 0, True)
-    step_a(0)
     step_a(1)
+    dispatch_plane(3)
+    for c in ow_copies:
+        c.wait_recv()
+    step_a(2)
+    begin((0, 1))
+    step_a(3)
     batch([(own_late, 0), (own_late, 1)])
-    step_a(2)
-    step_a(3)
     direct((0,))
     begin((2, 3))
+    step_b(0)
     batch(arrivals((0,), (-1, 1)))
+    step_b(1)
     relayed((0,))
     begin((4,))
     direct((1,))
-    ow_right.wait_recv()
-    on_right.start()
-    across_copies[0].start()
-    ow_left.wait_recv()
-    on_left.start()
-    across_copies[1].start()
-    step_b(0)
-    batch(arrivals((0,), (2,)) + arrivals((1,), (-1, 1)))
+    batch(arrivals((0,), (2,)))
+    step_b(2)
+    batch(arrivals((1,), (-1, 1)))
+    step_b(3)
     direct((2, 3))
-    step_b(1)
+    step_c(0)
     batch(arrivals((2,), (-1, 1)))
-    step_b(2)
+    step_c(2)
+    step_c(1)
     batch(arrivals((3,), (-1, 1)))
-    step_b(3)
+    step_c(3)
+    step_near(0)
+    step_near(2)
     relayed((1,))
     direct((4,))
-    on_right.wait_recv()
-    on_left.wait_recv()
-    across_copies[2].start()
-    step_c(0)
+    step_d(0)
+    step_d(2)
     batch(arrivals((1,), (2,)) + arrivals((4,), (-1, 1)))
+    step_near(1)
+    step_near(3)
     relayed((2, 3, 4))
-    step_c(1)
+    across.start()
+    step_d(1)
+    step_d(3)
     batch(arrivals((2,), (2,)) + arrivals((3,), (2,)) + arrivals((4,), (2,)))
-    step_c(2)
-    step_c(3)
-    step_d(0)
+    step_e(0)
+    step_e(2)
     unit(1, mirror, 0, False)
-    step_d(1)
     unit(1, mirror, 1, True)
-    step_d(2)
-    step_d(3)
 
     lam = lam_ref[core]
 
@@ -560,11 +573,10 @@
             else:
                 to_owner(1, n, 2 * mirror + 1).start()
 
-    for k in range(4):
-        step_e(k)
+    step_e(1)
+    step_e(3)
     keep_ow.wait()
-    for c in across_copies:
-        c.wait_recv()
+    across.wait_recv()
 
     for hd in range(8):
 
@@ -572,15 +584,19 @@
         def _(hd=hd):
             remote(heads.at[hd], heads.at[hd], head_send.at[0, 0], head_recv.at[hd], partner).wait_recv()
 
-    def project(n, carry):
-        at = pl.ds(pl.multiple_of(n * 512, 512), 512)
-        total = jnp.zeros((128, 512), f32)
-        for hd in range(8):
-            total = total + jnp.dot(heads[hd], ow[hd, :, at], preferred_element_type=f32)
+    def project(j, carry):
+        at = cols(j)
+        total = jnp.zeros((128, 128), f32)
+        for n in range(2):
+            total = total + jnp.dot(heads[2 * x + n], ow[n, :, at], preferred_element_type=f32)
+        for p in range(3):
+            other = 2 * wrap(x + 1 + p)
+            total = total + jnp.dot(heads[other + core], kv[j, p, 512:640, :], preferred_element_type=f32)
+            total = total + jnp.dot(heads[other + mate], ow_mate[j, p], preferred_element_type=f32)
         out_ref[:, at] = total.astype(bf16)
         return carry
 
-    lax.fori_loop(0, 4, project, 0)
+    lax.fori_loop(0, CHIPS, project, 0)
     step_f()
 
     give_kv.wait_send()
@@ -594,7 +610,7 @@
         far_q[0].wait_send()
         far_q[1].wait_send()
 
-    for c in sent + [ow_right, ow_left, on_right, on_left] + across_copies:
+    for c in sent + ow_copies + [across]:
         c.wait_send()
     for k, n in pairs[1:]:
         dispatch(k, n).wait_send()
@@ -625,14 +641,15 @@
         + [any_space] * 3,
         out_specs=(vmem, vmem),
         scratch_shapes=[
-            pltpu.VMEM((CHIPS, 4, 512, 128), bf16),
+            pltpu.VMEM((CHIPS, 4, 640, 128), bf16),
             pltpu.VMEM((2, 512, 128), bf16),
             pltpu.VMEM((2, 512, 128), bf16),
             pltpu.VMEM((2, 2, 128, 512), bf16),
             pltpu.VMEM((2, 2, 128, 512), f32),
             pltpu.VMEM((2, 2, 1, 512), f32),
             pltpu.VMEM((2, 2, 1, 512), f32),
-            pltpu.VMEM((8, 128, width), bf16),
+            pltpu.VMEM((2, 128, width), bf16),
+            pltpu.VMEM((CHIPS, 3, 128, 128), bf16),
             pltpu.VMEM((8, 128, 128), bf16),
             pltpu.VMEM((2, 512, 128), bf16),
             dma((3,)),
@@ -640,8 +657,8 @@
             dma((2,)),
             dma((2, 5, 4)),
             dma((2, 5, 4)),
-            dma((7,)),
-            dma((7,)),
+            dma((4,)),
+            dma((4,)),
             dma((2, 4)),
             dma((8,)),
             pltpu.VMEM((width, 256), bf16),
@@ -670,7 +687,7 @@
             dma((4, 8)),
             dma((4, 8)),
         ],
-        compiler_params=pltpu.CompilerParams(has_side_effects=True, vmem_limit_bytes=60 * 2**20),
+        compiler_params=pltpu.CompilerParams(collective_id=0, has_side_effects=True, vmem_limit_bytes=60 * 2**20),
         name="layer",
     )(
         query_rows,

time: 161 us -> 154 us (0.957)
  Pallas kernels: 153 us -> 145 us
    pallas_call x1, Pallas kernels: 153 us -> 145 us  [layer(): pl.pallas_call(layer_kernel, out_shape=(shape, shape), in_specs=[any_spac...]
where the time goes in v3:
time: 154 us
  Pallas kernels  145 us (94%)
  local copies, waits for them, and re-layouts  5.67 us (4%)
  other arithmetic  1.65 us (1%)
    pallas_call x1, Pallas kernels, layer(): pl.pallas_call(layer_kernel, out_shape=(shape, shape), in_specs=[any_spac...  145 us
    unnamed x11, local copies, waits for them, and re-layouts  4.19 us

profile of v3, /device:TPU:1, one launch (start us, length us, event | category | flops | bytes accessed | tf_op | source)
XLA Modules:
  0.0 153.5 jit_solution(2483163739013310680)
XLA Ops:
  0.6 0.0 copy-start.3
  0.6 0.6 copy-done.3
  1.3 0.0 copy-start.1
  1.3 0.7 copy-done.1
  2.0 0.1 copy.22
  2.1 0.1 broadcast_add_fusion
  2.2 0.1 eq.52
  2.3 0.1 eq.56
  2.5 0.6 reduce-window.6
  3.1 0.2 slice_reduce_fusion
  3.3 0.1 fusion.2
  3.4 0.1 reduce_sum.21
  3.5 0.1 multiply_add_fusion
  3.6 0.1 copy.24
  3.7 0.1 fusion
  3.8 0.0 copy-start.2
  3.8 0.7 convert_element_type.9.place_ref
  4.4 0.0 copy-done.2
  4.5 0.8 copy.26.mix_ref
  5.3 145.5 %layer.1 = (bf16[128,2048]{1,0:T(8,128)(2,1)}, bf16[128,2048]{1,0:T(8,128)(2,1)}) custom-call(bf16[512,256]{1,0:T(8,128)(2,1)} %q_ref.1, bf16[512,256]{1,0:T(8,128)(2,1)} %k_ref.1, bf16[512,256]{1,0:T(8,128)(2,1)} %v_ref.1, f32[2]{0:T(128)} %lam_ref.1, f32[1,128]{1,0:T(1,128)} %bitcast.26, bf16[2,128,2048]{2,1,0:T(8,128)(2,1)} %bitcast.21, ...), custom_call_target="tpu_custom_call" | custom-call | tf_op jit(solution)/shard_map/layer/pallas_call | solution.py:636
  150.8 0.0 copy-start
  150.8 1.9 %copy.31 = bf16[128,2048]{1,0:T(8,128)(2,1)} copy(bf16[128,2048]{1,0:T(8,128)(2,1)} %get-tuple-element.4) | data formatting | bytes 1048576
  152.7 0.0 copy-done
  152.7 0.8 copy.32
  (5 shorter events, 0.1 us)
Async XLA Ops:
  0.6 0.7 copy-start.3
  1.3 0.7 copy-start.1
  3.8 0.7 copy-start.2
  150.8 2.0 %copy-start = (bf16[128,2048]{1,0:T(8,128)(2,1)S(1)}, bf16[128,2048]{1,0:T(8,128)(2,1)}, u32[]{:S(2)}) copy-start(bf16[128,2048]{1,0:T(8,128)(2,1)} %get-tuple-element.5) | copy-start | bytes 1572868
